TPU v7x, 256 devices: a whole 4x4x8 slice. The times are simulated.
256 devices in a mesh: sp: 16 (over y, x), tp: 16 (over z, core).
Axes of the slice: x: 4, y: 4, z: 8, core: 2. Of those that a mesh axis runs over, the one named last changes fastest.
Arguments:
- queries: bfloat16 [16384, 1024], P('sp', 'tp'), may hold values from -18 to 18
- keys: bfloat16 [16384, 256], P('sp'), may hold values from -18 to 18
- values: bfloat16 [16384, 256], P('sp'), may hold values from -6 to 6
- sink_logits: float32 [16], P('tp'), may hold values from 3 to 7
- w_out: bfloat16 [1024, 2048], P('tp'), may hold values from -1.5 to 1.5
- residual: bfloat16 [16384, 2048], P(('sp', 'tp')), may hold values from -6 to 6
- norm_gain: float32 [2048], replicated, may hold values from 0.1 to 1.9
- expert_ids: int32 [16384, 4], P('sp'), may hold values from 0 to 127, all different within a row; in each aligned block of 1024 rows (0 to 1023, 1024 to 2047, ...) at most 64 rows name the same one
- expert_weights: float32 [16384, 4], P('sp'), may hold values from 0.1 to 1.5
- w_gate: bfloat16 [256, 768, 2048], P(('sp', 'tp')), may hold values from -0.125 to 0.125
- w_up: bfloat16 [256, 768, 2048], P(('sp', 'tp')), may hold values from -0.125 to 0.125
- w_down: bfloat16 [256, 768, 2048], P(('sp', 'tp')), may hold values from -0.15625 to 0.15625
- shared_gate: bfloat16 [512, 2048], P('tp'), may hold values from -0.125 to 0.125
- shared_up: bfloat16 [512, 2048], P('tp'), may hold values from -0.125 to 0.125
- shared_down: bfloat16 [512, 2048], P('tp'), may hold values from -0.25 to 0.25
Outputs:
- layer_out: bfloat16 [16384, 2048], P(('sp', 'tp'))
Inputs may be any that keep to these rules, and one draw needn't show every extreme that they name: `expert_ids`: each row names 4 different experts; in each aligned block of 1024 rows no expert is named by more than 64 rows.
All inputs are finite; a program needn't handle non-finite values.
Results may differ from a plain program's by a relative error of at most 0.02.
Values may be sent and summed in bfloat16 or wider, within the bound.
A program may use at most 128 MiB of HBM per device.

v0:
```python
import jax
import jax.numpy as jnp
from jax import lax
from jax.sharding import PartitionSpec as P

HD = 64
GROUP = 4
WINDOW = 128
TOPK = 4


def shifted(block, axis, distance):
    devices = range(lax.axis_size(axis))
    route = [(i - distance, i) for i in devices if i - distance in devices]
    return lax.ppermute(block, axis, route)


def from_partner(x, axis, apart):
    return lax.ppermute(x, axis, [(i, i ^ 1 << apart) for i in range(lax.axis_size(axis))])


def normalize(after_mix, norm_gain):
    values_f = after_mix.astype(jnp.float32)
    scale = lax.rsqrt(jnp.mean(values_f * values_f, axis=-1, keepdims=True) + 1e-06)
    return (values_f * scale * norm_gain).astype(jnp.bfloat16)


def slot_layout(route_ids, expert_count, capacity):
    flat_ids = route_ids.reshape(-1)
    matches = (flat_ids[:, None] == jnp.arange(expert_count, dtype=jnp.int32)[None, :]).astype(
        jnp.int32
    )
    earlier = jnp.cumsum(matches, axis=0) - matches
    order_in = jnp.sum(earlier * matches, axis=1)
    slot_index = flat_ids * capacity + order_in
    owners = jnp.arange(flat_ids.shape[0], dtype=jnp.int32) // TOPK
    slot_owner = jnp.full((expert_count * capacity,), -1, jnp.int32).at[slot_index].set(owners)
    return (slot_index, slot_owner)


def body(
    queries,
    keys,
    values,
    sink_logits,
    w_out,
    residual,
    norm_gain,
    expert_ids,
    expert_weights,
    w_gate,
    w_up,
    w_down,
    shared_gate,
    shared_up,
    shared_down,
):
    tp_count = lax.axis_size("tp")
    sp_count = lax.axis_size("sp")
    seq_rows = queries.shape[0]
    expert_count = sp_count * tp_count // 2
    capacity = max(2, 2 * seq_rows * TOPK // expert_count)
    local_heads = queries.shape[1] // HD
    kv_start = lax.axis_index("tp") * local_heads // GROUP * HD
    key_cols = lax.dynamic_slice_in_dim(keys, kv_start, HD, 1)
    value_cols = lax.dynamic_slice_in_dim(values, kv_start, HD, 1)
    rim_keys, rim_values = shifted(
        (key_cols[seq_rows - WINDOW :], value_cols[seq_rows - WINDOW :]), "sp", 1
    )
    num_blocks = seq_rows // WINDOW
    key_blocks = key_cols.reshape(num_blocks, WINDOW, HD)
    value_blocks = value_cols.reshape(num_blocks, WINDOW, HD)
    keys_ext = jnp.concatenate(
        [jnp.concatenate([rim_keys[None], key_blocks[:-1]], axis=0), key_blocks], axis=1
    )
    values_ext = jnp.concatenate(
        [jnp.concatenate([rim_values[None], value_blocks[:-1]], axis=0), value_blocks], axis=1
    )
    query_blocks = queries.reshape(num_blocks, WINDOW, local_heads, HD)
    scores = jnp.einsum(
        "nqhd,nsd->nhqs", query_blocks, keys_ext, preferred_element_type=jnp.float32
    ) * HD ** (-0.5)
    query_pos = jnp.arange(WINDOW)[:, None] + WINDOW
    key_pos = jnp.arange(2 * WINDOW)[None, :]
    in_band = (key_pos <= query_pos) & (key_pos > query_pos - WINDOW)
    absolute = (
        lax.axis_index("sp") * seq_rows
        + jnp.arange(num_blocks)[:, None, None] * WINDOW
        + key_pos[None]
        - WINDOW
    )
    allowed = in_band[None] & (absolute >= 0)
    scores = jnp.where(allowed[:, None], scores, -jnp.inf)
    sink_col = jnp.broadcast_to(sink_logits[None, :, None, None], scores.shape[:-1] + (1,))
    combined = jnp.concatenate([scores, sink_col], axis=-1)
    row_max = jnp.max(combined, axis=-1, keepdims=True)
    exps = jnp.exp(combined - row_max)
    weights = (exps[..., :-1] / jnp.sum(exps, axis=-1, keepdims=True)).astype(jnp.bfloat16)
    attended = jnp.einsum("nhqs,nsd->nqhd", weights, values_ext, preferred_element_type=jnp.float32)
    attended = attended.astype(jnp.bfloat16).reshape(seq_rows, local_heads * HD)
    head_rows = lax.all_to_all(attended, "tp", split_axis=0, concat_axis=1, tiled=True)
    projected = jnp.dot(
        head_rows,
        lax.all_gather(w_out, "tp", axis=0, tiled=True),
        preferred_element_type=jnp.float32,
    )
    after_mix = (residual.astype(jnp.float32) + projected).astype(jnp.bfloat16)
    normed = normalize(after_mix, norm_gain)
    tp_index = lax.axis_index("tp")
    lanes = tp_count // 2
    lane = tp_index // 2
    keep = tp_index % 2
    half_cap = capacity // 2
    slot_index, slot_owner = slot_layout(expert_ids, expert_count, capacity)
    all_rows = lax.all_gather(normed, "tp", axis=0, tiled=True)
    lane_owner = lax.dynamic_slice_in_dim(slot_owner.reshape(sp_count, lanes, capacity), lane, 1, 1)
    lane_owner = lane_owner.reshape(sp_count * capacity)
    picked = all_rows[jnp.maximum(lane_owner, 0)]
    outgoing = jnp.where((lane_owner >= 0)[:, None], picked, jnp.zeros((), jnp.bfloat16))
    arrived = lax.all_to_all(
        outgoing.reshape(sp_count, capacity, -1), "sp", split_axis=0, concat_axis=0, tiled=True
    )
    arrived = arrived.reshape(sp_count * capacity, -1)
    gate_act = jnp.einsum("td,fd->tf", arrived, w_gate[0], preferred_element_type=jnp.float32)
    up_act = jnp.einsum("td,fd->tf", arrived, w_up[0], preferred_element_type=jnp.float32)
    hidden = (jax.nn.silu(gate_act) * up_act).astype(jnp.bfloat16)
    half_out = jnp.dot(hidden, w_down[0], preferred_element_type=jnp.float32).astype(jnp.bfloat16)
    half_out = half_out.reshape(sp_count, 2, half_cap, -1)
    mine = lax.dynamic_index_in_dim(half_out, keep, 1, keepdims=False)
    other = lax.dynamic_index_in_dim(half_out, 1 - keep, 1, keepdims=False)
    partner = from_partner(other, "tp", 0)
    expert_sum = (mine.astype(jnp.float32) + partner.astype(jnp.float32)).astype(jnp.bfloat16)
    held = lax.all_to_all(expert_sum, "sp", split_axis=0, concat_axis=0, tiled=True).reshape(
        sp_count * half_cap, -1
    )
    route_rank = slot_index.reshape(seq_rows, TOPK) - expert_ids * capacity
    held_here = (expert_ids % lanes == lane) & (route_rank // half_cap == keep)
    position = expert_ids // lanes * half_cap + route_rank % half_cap
    scaled = jnp.where(held_here, expert_weights, jnp.zeros((), expert_weights.dtype))
    shared_gate_act = jnp.einsum(
        "td,fd->tf", all_rows, shared_gate, preferred_element_type=jnp.float32
    )
    shared_up_act = jnp.einsum("td,fd->tf", all_rows, shared_up, preferred_element_type=jnp.float32)
    shared_hidden = (jax.nn.silu(shared_gate_act) * shared_up_act).astype(jnp.bfloat16)
    partial_sum = jnp.dot(shared_hidden, shared_down, preferred_element_type=jnp.float32)
    for route_slot in range(TOPK):
        partial_sum = partial_sum + scaled[:, route_slot : route_slot + 1] * held[
            position[:, route_slot]
        ].astype(jnp.float32)
    moe_sum = lax.psum_scatter(
        partial_sum.astype(jnp.bfloat16), "tp", scatter_dimension=0, tiled=True
    )
    return (after_mix.astype(jnp.float32) + moe_sum.astype(jnp.float32)).astype(jnp.bfloat16)


def solution(mesh):
    return jax.shard_map(
        body,
        mesh=mesh,
        in_specs=(
            P("sp", "tp"),
            P("sp", None),
            P("sp", None),
            P("tp"),
            P("tp", None),
            P(("sp", "tp"), None),
            P(),
            P("sp", None),
            P("sp", None),
            P(("sp", "tp"), None, None),
            P(("sp", "tp"), None, None),
            P(("sp", "tp"), None, None),
            P("tp", None),
            P("tp", None),
            P("tp", None),
        ),
        out_specs=P(("sp", "tp"), None),
        check_vma=False,
    )
```

profile of v0, /device:TPU:1, one launch (start us, length us, event | category | flops | bytes accessed | tf_op | source)
XLA Modules:
  0.0 359.2 jit_solution(7965205949438890940)
XLA Ops:
  7.3 2.1 constant_dynamic-slice_fusion
  9.6 3.9 %collective-permute-start.1 = (bf16[128,64]{0,1:T(8,128)(2,1)S(1)}, bf16[128,64]{0,1:T(8,128)(2,1)S(1)}, u32[]{:S(2)}, u32[]{:S(2)}) collective-permute-start(bf16[128,64]{0,1:T(8,128)(2,1)S(1)} %slice.80), channel_id=1, source_target_pairs={{0,16},{16,32},{32,48},{48,64},{64,80},{80,96},{96,112},{112,128},... | collective-permute-start | bytes 49160 | tf_op jit(solution)/shard_map/ppermute | solution.py:15
  13.5 1.1 copy.93
  14.6 3.1 collective-permute-start
  18.7 1.5 fusion.15
  21.7 1.2 reshape.297
  22.9 19.9 %all_to_all.29 = bf16[16,2,2048]{2,1,0:T(2,128)(2,1)S(1)} all-to-all(bf16[16,2,2048]{2,1,0:T(2,128)(2,1)S(1)} %reshape.297), channel_id=1, replica_groups=mesh['sp'=16,'tp'=16] {'tp'}, dimensions={0} | all-to-all | bytes 262144 | tf_op jit(solution)/shard_map/all_to_all | solution.py:101
  43.1 14.4 %all-gather.3.cloned.1.call-done = bf16[1024,2048]{1,0:T(8,128)(2,1)} async-done(((bf16[64,2048]{1,0:T(8,128)(2,1)}), bf16[1024,2048]{1,0:T(8,128)(2,1)}) %all-gather.3.cloned.1.call-update) | async-done | bytes 4194320 | tf_op jit(solution)/shard_map/all_gather | solution.py:104
  57.4 3.2 multiply_reduce_fusion
  60.6 0.8 copy-done.5
  61.4 0.8 multiply_convert_fusion.1
  62.3 1.0 copy.78
  63.3 1.3 eq.48
  64.6 1.3 eq.44
  66.0 1.0 copy.87
  67.0 1.4 mul.144
  69.1 1.3 copy-done.4
  70.5 1.8 broadcast_add_fusion
  72.3 1.2 copy.85
  73.5 1.4 fusion.11
  75.0 15.5 %scatter_custom_fusion = s32[8192]{0:T(1024)S(1)} fusion(s32[4096]{0:T(1024)S(1)} %bitcast.113, s32[4096]{0:T(1024)S(1)} %add_select_fusion.4, s32[]{:T(128)} %constant.133.clone.1), kind=kCustom, calls=%fused_computation.114 | custom fusion | bytes 32772 | tf_op jit(solution)/shard_map/scatter | solution.py:37
  90.8 12.3 %all-gather.5.cloned.1.call-done = bf16[1024,2048]{1,0:T(8,128)(2,1)} async-done(((bf16[64,2048]{1,0:T(8,128)(2,1)}), bf16[1024,2048]{1,0:T(8,128)(2,1)}) %all-gather.5.cloned.1.call-update) | async-done | bytes 4194320 | tf_op jit(solution)/shard_map/all_gather | solution.py:115
  103.1 11.6 %gather_fusion = bf16[1024,2048]{1,0:T(8,128)(2,1)} fusion(bf16[1024,2048]{1,0:T(8,128)(2,1)} %all-gather.5.cloned.1.call-done, s32[1024]{0:T(1024)S(1)} %broadcast_clamp_fusion.4), kind=kCustom, calls=%fused_computation | custom fusion | bytes 8392704 | tf_op jit(solution)/shard_map/gather | solution.py:118
  114.6 4.5 %broadcast_select_fusion = bf16[16,64,2048]{2,1,0:T(8,128)(2,1)} fusion(bf16[16,64,2048]{2,1,0:T(8,128)(2,1)} %bitcast.107, pred[16,64]{1,0:T(8,128)(4,1)S(1)} %bitcast.114), kind=kLoop, calls=%fused_computation.9 | loop fusion | flops 2097152 | bytes 8389632 | tf_op jit(solution)/shard_map/jit(_where)/select_n | solution.py:119
  119.1 6.6 %all-to-all-start.1 = ((bf16[16,64,2048]{2,1,0:T(8,128)(2,1)}), bf16[16,64,2048]{2,1,0:T(8,128)(2,1)}, u32[]{:S(2)}, u32[]{:S(2)}) async-start(bf16[16,64,2048]{2,1,0:T(8,128)(2,1)} %broadcast_select_fusion), calls=%async_computation.1 | async-start | bytes 8388608 | tf_op jit(solution)/shard_map/all_to_all | solution.py:120
  125.7 62.8 %all-to-all-done.1 = bf16[16,64,2048]{2,1,0:T(8,128)(2,1)} async-done(((bf16[16,64,2048]{2,1,0:T(8,128)(2,1)}), bf16[16,64,2048]{2,1,0:T(8,128)(2,1)}, u32[]{:S(2)}, u32[]{:S(2)}) %all-to-all-start.1) | async-done | bytes 4194336 | tf_op jit(solution)/shard_map/all_to_all | solution.py:120
  188.6 8.3 %fusion.2 = f32[1024,768]{1,0:T(8,128)} fusion(bf16[1024,2048]{1,0:T(8,128)(2,1)} %bitcast.16, bf16[1,768,2048]{2,1,0:T(8,128)(2,1)} %param.25), kind=kOutput, calls=%fused_computation.12 | convolution fusion | flops 3221225472 | bytes 10485760 | tf_op jit(solution)/shard_map/td,fd->tf/dot_general | solution.py:125
  196.9 12.4 %convolution_convert_fusion = bf16[1024,2048]{1,0:T(8,128)(2,1)} fusion(bf16[1,768,2048]{2,1,0:T(8,128)(2,1)S(1)} %copy-done, f32[1024,768]{1,0:T(8,128)} %fusion.2, bf16[1024,2048]{1,0:T(8,128)(2,1)} %bitcast.16, bf16[1,768,2048]{2,1,0:T(8,128)(2,1)} %param.24), kind=kOutput, calls=%fused_computation.10 | convolution fusion | flops 6449266688 | bytes 17825792 | tf_op jit(solution)/shard_map/dot_general | solution.py:127
  209.3 3.2 dynamic-slice_bitcast_fusion
  212.5 1.4 collective-permute-start.2
  213.9 4.0 %collective-permute-done.2 = bf16[16,32,2048]{2,1,0:T(8,128)(2,1)S(1)} collective-permute-done((bf16[16,32,2048]{2,1,0:T(8,128)(2,1)}, bf16[16,32,2048]{2,1,0:T(8,128)(2,1)S(1)}, u32[]{:S(2)}, u32[]{:S(2)}) %collective-permute-start.2) | collective-permute-done | bytes 2097184 | tf_op jit(solution)/shard_map/ppermute | solution.py:19
  217.9 3.9 %fusion = bf16[16,32,2048]{2,1,0:T(8,128)(2,1)} fusion(bf16[16,32,2048]{2,1,0:T(8,128)(2,1)S(1)} %collective-permute-done.2, bf16[16,2,32,2048]{3,2,1,0:T(8,128)(2,1)} %bitcast.109, s32[]{:T(128)S(6)} %select_n.103), kind=kLoop, calls=%fused_computation.8 | loop fusion | flops 4194304 | bytes 6291460 | tf_op jit(solution)/shard_map/convert_element_type | solution.py:132
  221.8 4.9 %all-to-all-start.2 = ((bf16[16,32,2048]{2,1,0:T(8,128)(2,1)}), bf16[16,32,2048]{2,1,0:T(8,128)(2,1)S(1)}, u32[]{:S(2)}, u32[]{:S(2)}) async-start(bf16[16,32,2048]{2,1,0:T(8,128)(2,1)} %fusion), calls=%async_computation.2 | async-start | bytes 4194304 | tf_op jit(solution)/shard_map/all_to_all | solution.py:133
  227.0 1.3 reduce_sum.34
  228.6 1.1 copy.86
  229.7 1.9 fusion.35
  231.6 1.0 slice_reduce_fusion.3
  232.6 1.6 fusion.25
  234.2 1.0 fusion.26
  235.3 1.3 fusion.67
  236.6 22.2 %all-to-all-done.2 = bf16[16,32,2048]{2,1,0:T(8,128)(2,1)S(1)} async-done(((bf16[16,32,2048]{2,1,0:T(8,128)(2,1)}), bf16[16,32,2048]{2,1,0:T(8,128)(2,1)S(1)}, u32[]{:S(2)}, u32[]{:S(2)}) %all-to-all-start.2) | async-done | bytes 2097184 | tf_op jit(solution)/shard_map/all_to_all | solution.py:133
  258.8 6.0 %gather_fusion.4 = bf16[1024,2048]{1,0:T(8,128)(2,1)} fusion(bf16[512,2048]{1,0:T(8,128)(2,1)S(1)} %bitcast.103, s32[1024]{0:T(1024)S(1)} %get-tuple-element.19), kind=kCustom, calls=%fused_computation.4 | custom fusion | bytes 8392704 | tf_op jit(solution)/shard_map/gather | solution.py:147
  264.8 6.0 %gather_fusion.3 = bf16[1024,2048]{1,0:T(8,128)(2,1)} fusion(bf16[512,2048]{1,0:T(8,128)(2,1)S(1)} %bitcast.104, s32[1024]{0:T(1024)S(1)} %get-tuple-element.20), kind=kCustom, calls=%fused_computation.3 | custom fusion | bytes 8392704 | tf_op jit(solution)/shard_map/gather | solution.py:147
  270.8 6.1 %gather_fusion.2 = bf16[1024,2048]{1,0:T(8,128)(2,1)} fusion(bf16[512,2048]{1,0:T(8,128)(2,1)S(1)} %bitcast.105, s32[1024]{0:T(1024)S(1)} %get-tuple-element.21), kind=kCustom, calls=%fused_computation.2 | custom fusion | bytes 8392704 | tf_op jit(solution)/shard_map/gather | solution.py:147
  276.9 6.0 %gather_fusion.1 = bf16[1024,2048]{1,0:T(8,128)(2,1)} fusion(bf16[512,2048]{1,0:T(8,128)(2,1)S(1)} %bitcast.106, s32[1024]{0:T(1024)S(1)} %get-tuple-element.22), kind=kCustom, calls=%fused_computation.1 | custom fusion | bytes 8392704 | tf_op jit(solution)/shard_map/gather | solution.py:147
  282.9 11.2 %add_convert_fusion = bf16[1024,2048]{1,0:T(8,128)(2,1)} fusion(bf16[1024,2048]{1,0:T(8,128)(2,1)} %gather_fusion.4, bf16[1024,2048]{1,0:T(8,128)(2,1)} %gather_fusion.3, bf16[1024,2048]{1,0:T(8,128)(2,1)} %gather_fusion.2, bf16[1024,2048]{1,0:T(8,128)(2,1)} %gather_fusion.1, bf16[32,2048]{1,0:T(8,128)(2,1)S(1)} %copy-done.10, ...), kind=kOutput, calls=%fused_computation.6 | convolution fusion | flops 295895040 | bytes 25575424 | tf_op jit(solution)/shard_map/dot_general | solution.py:145
  294.2 56.6 %reduce-scatter.2.cloned.1.call-done = bf16[64,2048]{1,0:T(8,128)(2,1)} async-done(((bf16[1024,2048]{1,0:T(8,128)(2,1)}), bf16[64,2048]{1,0:T(8,128)(2,1)}) %reduce-scatter.2.cloned.1.call-update) | async-done | bytes 262160 | tf_op jit(solution)/shard_map/reduce_scatter | solution.py:150
  350.8 1.9 add_convert_fusion.1
  (67 shorter events, 4.4 us)
Async XLA Ops:
  6.5 190.3 %copy-start = (bf16[1,768,2048]{2,1,0:T(8,128)(2,1)S(1)}, bf16[1,768,2048]{2,1,0:T(8,128)(2,1)}, u32[]{:S(2)}) copy-start(bf16[1,768,2048]{2,1,0:T(8,128)(2,1)} %param.26) | copy-start | bytes 9437188
  6.5 50.9 %all-gather.3.cloned.1.call-start = ((), (), s32[]{:S(2)}) async-start(), calls=%async_computation.4 | async-start | bytes 4456448 | tf_op jit(solution)/shard_map/all_gather | solution.py:104
  7.3 95.8 %all-gather.5.cloned.1.call-start = ((), (), s32[]{:S(2)}) async-start(), calls=%async_computation.5 | async-start | bytes 4456448 | tf_op jit(solution)/shard_map/all_gather | solution.py:115
  9.6 9.1 %collective-permute-start.1 = (bf16[128,64]{0,1:T(8,128)(2,1)S(1)}, bf16[128,64]{0,1:T(8,128)(2,1)S(1)}, u32[]{:S(2)}, u32[]{:S(2)}) collective-permute-start(bf16[128,64]{0,1:T(8,128)(2,1)S(1)} %slice.80), channel_id=1, source_target_pairs={{0,16},{16,32},{32,48},{48,64},{64,80},{80,96},{96,112},{112,128},... | collective-permute-start | bytes 49160 | tf_op jit(solution)/shard_map/ppermute | solution.py:15
  14.6 5.8 %collective-permute-start = (bf16[128,64]{0,1:T(8,128)(2,1)S(1)}, bf16[128,64]{0,1:T(8,128)(2,1)S(1)}, u32[]{:S(2)}, u32[]{:S(2)}) collective-permute-start(bf16[128,64]{0,1:T(8,128)(2,1)S(1)} %slice.78), channel_id=1, source_target_pairs={{0,16},{16,32},{32,48},{48,64},{64,80},{80,96},{96,112},{112,128},... | collective-permute-start | bytes 49160 | tf_op jit(solution)/shard_map/ppermute | solution.py:15
  20.8 41.5 %copy-start.6 = (s32[1024,4]{0,1:T(4,128)S(1)}, s32[1024,4]{0,1:T(4,128)}, u32[]{:S(2)}) copy-start(s32[1024,4]{0,1:T(4,128)} %param.22) | copy-start | bytes 49156
  43.1 18.4 %copy-start.9 = (f32[2048]{0:T(1024)S(1)}, f32[2048]{0:T(1024)}, u32[]{:S(2)}) copy-start(f32[2048]{0:T(1024)} %param.21) | copy-start | bytes 24580
  60.6 0.8 copy-start.5
  69.1 1.3 copy-start.4
  119.1 69.4 %all-to-all-start.1 = ((bf16[16,64,2048]{2,1,0:T(8,128)(2,1)}), bf16[16,64,2048]{2,1,0:T(8,128)(2,1)}, u32[]{:S(2)}, u32[]{:S(2)}) async-start(bf16[16,64,2048]{2,1,0:T(8,128)(2,1)} %broadcast_select_fusion), calls=%async_computation.1 | async-start | bytes 8388608 | tf_op jit(solution)/shard_map/all_to_all | solution.py:120
  212.5 5.4 %collective-permute-start.2 = (bf16[16,32,2048]{2,1,0:T(8,128)(2,1)}, bf16[16,32,2048]{2,1,0:T(8,128)(2,1)S(1)}, u32[]{:S(2)}, u32[]{:S(2)}) collective-permute-start(bf16[16,32,2048]{2,1,0:T(8,128)(2,1)} %dynamic-slice_bitcast_fusion), channel_id=1, source_target_pairs={{0,1},{1,0},{2,3},{3,2},{4,5},{5,4},{6,7},{7,6},{8,9},{9,8},{10,11... | collective-permute-start | bytes 6291464 | tf_op jit(solution)/shard_map/ppermute | solution.py:19
  213.9 14.7 %copy-start.8 = (f32[1024,4]{0,1:T(4,128)S(1)}, f32[1024,4]{0,1:T(4,128)}, u32[]{:S(2)}) copy-start(f32[1024,4]{0,1:T(4,128)} %param.23) | copy-start | bytes 49156
  221.8 7.9 %copy-start.3 = (s32[1024,4]{1,0:T(8,128)S(1)}, s32[1024,4]{1,0:T(8,128)}, u32[]{:S(2)}) copy-start(s32[1024,4]{1,0:T(8,128)} %copy.78) | copy-start | bytes 49156
  221.8 37.0 %all-to-all-start.2 = ((bf16[16,32,2048]{2,1,0:T(8,128)(2,1)}), bf16[16,32,2048]{2,1,0:T(8,128)(2,1)S(1)}, u32[]{:S(2)}, u32[]{:S(2)}) async-start(bf16[16,32,2048]{2,1,0:T(8,128)(2,1)} %fusion), calls=%async_computation.2 | async-start | bytes 4194304 | tf_op jit(solution)/shard_map/all_to_all | solution.py:133
  226.7 124.1 %reduce-scatter.2.cloned.1.call-start = ((), (), s32[]{:S(2)}) async-start(), calls=%async_computation.6 | async-start | bytes 4456448 | tf_op jit(solution)/shard_map/reduce_scatter | solution.py:150
  229.7 5.6 %copy-start.2 = (bf16[1024,2048]{1,0:T(8,128)(2,1)S(1)}, bf16[1024,2048]{1,0:T(8,128)(2,1)}, u32[]{:S(2)}) copy-start(bf16[1024,2048]{1,0:T(8,128)(2,1)} %all-gather.5.cloned.1.call-done) | copy-start | bytes 12582916
  229.7 5.6 %copy-start.7 = (bf16[32,2048]{1,0:T(8,128)(2,1)S(1)}, bf16[32,2048]{1,0:T(8,128)(2,1)}, u32[]{:S(2)}) copy-start(bf16[32,2048]{1,0:T(8,128)(2,1)} %param.27) | copy-start | bytes 393220
  276.9 6.0 %copy-start.10 = (bf16[32,2048]{1,0:T(8,128)(2,1)S(1)}, bf16[32,2048]{1,0:T(8,128)(2,1)}, u32[]{:S(2)}) copy-start(bf16[32,2048]{1,0:T(8,128)(2,1)} %param.29) | copy-start | bytes 393220
  276.9 6.0 %copy-start.11 = (bf16[32,2048]{1,0:T(8,128)(2,1)S(1)}, bf16[32,2048]{1,0:T(8,128)(2,1)}, u32[]{:S(2)}) copy-start(bf16[32,2048]{1,0:T(8,128)(2,1)} %param.28) | copy-start | bytes 393220
  282.9 69.7 %copy-start.1 = (bf16[1,768,2048]{2,1,0:T(8,128)(2,1)S(1)}, bf16[1,768,2048]{2,1,0:T(8,128)(2,1)}, u32[]{:S(2)}) copy-start(bf16[1,768,2048]{2,1,0:T(8,128)(2,1)} %param.26) | copy-start | bytes 9437188
Sparse Core Ops, SparseCore 0:
  9.2 48.2 all-gather.2
  62.4 40.6 all-gather.4
  294.3 56.4 reduce-scatter.1
where the time goes:
time: 362 us; the launch traced here: 359 us
  waiting for transfers between devices  173 us (48%)
  local copies, waits for them, and re-layouts  73.6 us (20%)
  matrix products  38.2 us (11%)
  starting transfers between devices  20.2 us (6%)
  other arithmetic  20 us (6%)
  blocking collectives  19.9 us (5%)
  between operations  14.2 us (4%)
    all_to_all x1, waiting for transfers between devices, body(): lax.all_to_all(outgoing.reshape(sp_count, capacity, -1), 'sp', split_axis...  62.8 us
    reduce_scatter x1, waiting for transfers between devices, body(): lax.psum_scatter(partial_sum.astype(jnp.bfloat16), 'tp', scatter_dimensio...  56.6 us
    gather x4, local copies, waits for them, and re-layouts, body(): held[position[:, route_slot]].astype(jnp.float32)  24.1 us
    all_to_all x1, waiting for transfers between devices, body(): lax.all_to_all(expert_sum, 'sp', split_axis=0, concat_axis=0, tiled=True)  22.2 us
    all_to_all x1, blocking collectives, body(): lax.all_to_all(attended, 'tp', split_axis=0, concat_axis=1, tiled=True)  19.9 us
    scatter x1, local copies, waits for them, and re-layouts, slot_layout(): jnp.full((expert_count * capacity,), -1, jnp.int32).at[slot_index]  15.5 us
    all_gather x1, waiting for transfers between devices, body(): lax.all_gather(w_out, 'tp', axis=0, tiled=True)  14.4 us
    dot_general x1, matrix products, body(): jnp.dot(hidden, w_down[0], preferred_element_type=jnp.float32)  12.4 us
  transfers between devices with their start and end apart: 8, of which 6 were waited for; matrix products, arithmetic and copies ran while one was open for 12% of the time, Pallas kernels for 0%

commit v1 on v0

v1 whole, which is shorter than its diff:
```python
import jax
import jax.numpy as jnp
from jax import lax
from jax.experimental import pallas as pl
from jax.experimental.pallas import tpu as pltpu
from jax.sharding import PartitionSpec as P

HD = 64
GROUP = 4
WINDOW = 128
TOPK = 4


def shifted(block, axis, distance):
    devices = range(lax.axis_size(axis))
    route = [(i - distance, i) for i in devices if i - distance in devices]
    return lax.ppermute(block, axis, route)


def normalize(after_mix, norm_gain):
    values_f = after_mix.astype(jnp.float32)
    scale = lax.rsqrt(jnp.mean(values_f * values_f, axis=-1, keepdims=True) + 1e-06)
    return (values_f * scale * norm_gain).astype(jnp.bfloat16)


MESH = pl.DeviceIdType.MESH
CHUNKS = 4
CAP = 64


def dot_nt(a, b):
    return lax.dot_general(a, b, (((1,), (1,)), ((), ())), preferred_element_type=jnp.float32)


def dot_nn(a, b):
    return jnp.dot(a, b, preferred_element_type=jnp.float32)


def rows_loop(total, step, fn):
    def one(i, carry):
        fn(pl.ds(pl.multiple_of(i * step, step), step))
        return carry

    lax.fori_loop(0, total // step, one, 0)


class Place:
    def __init__(self):
        self.sp_count = lax.axis_size("sp")
        self.tp_count = lax.axis_size("tp")
        self.s = lax.axis_index("sp")
        self.t = lax.axis_index("tp")
        self.c = self.t % 2
        self.z = self.t // 2
        self.nz = self.tp_count // 2
        self.partner = (self.s, self.t + 1 - 2 * self.c)
        self.right = (self.s, (self.t + 2) % self.tp_count)
        self.left = (self.s, (self.t + self.tp_count - 2) % self.tp_count)

    def peer(self, o):
        return ((self.s + o) % self.sp_count, self.t)

    def barrier(self, devices, peers=True):
        sem = pltpu.get_barrier_semaphore()
        for device in devices:
            pl.semaphore_signal(sem, inc=1, device_id=device, device_id_type=MESH)
        count = len(devices)
        if peers:

            def one(o, carry):
                pl.semaphore_signal(sem, inc=1, device_id=self.peer(o), device_id_type=MESH)
                return carry

            lax.fori_loop(1, self.sp_count, one, 0)
            count += self.sp_count - 1
        pl.semaphore_wait(sem, count)

    def steps(self, j):
        far, near = self.nz // 2, self.nz - 1 - self.nz // 2
        return (far, near) if j % 2 == 0 else (near, far)


def remote(src, dst, send_sem, recv_sem, device):
    return pltpu.make_async_remote_copy(
        src_ref=src, dst_ref=dst, send_sem=send_sem, recv_sem=recv_sem, device_id=device, device_id_type=MESH
    )


class RingGather:
    def __init__(self, p, buf, rows, send_sems, recv_sems):
        self.p, self.buf, self.rows = p, buf, rows
        self.ss, self.rs = send_sems, recv_sems

    def copy(self, j, way, k, shift):
        p = self.p
        origin = (p.z - shift if way == 0 else p.z + shift) + p.nz
        block = self.buf.at[j, pl.ds(pl.multiple_of(origin % p.nz * self.rows, self.rows), self.rows)]
        return remote(block, block, self.ss.at[j, way, k - 1], self.rs.at[j, way, k - 1], p.left if way else p.right)

    def send(self, j, k):
        for way in range(2):
            if k <= self.p.steps(j)[way]:
                self.copy(j, way, k, k - 1).start()

    def wait(self, j, k):
        for way in range(2):
            if k <= self.p.steps(j)[way]:
                self.copy(j, way, k, k).wait_recv()

    def drain(self, j):
        for way in range(2):
            for k in range(1, self.p.steps(j)[way] + 1):
                self.copy(j, way, k, k - 1).wait_send()


class Exchange:
    def __init__(self, p, src, dst, rows, send_sems, recv_sems):
        self.p, self.src, self.dst, self.rows = p, src, dst, rows
        self.ss, self.rs = send_sems, recv_sems

    def block(self, index):
        return pl.ds(pl.multiple_of(index * self.rows, self.rows), self.rows)

    def send(self, j):
        p = self.p

        def one(o, carry):
            peer = p.peer(o)
            remote(
                self.src.at[j, self.block(peer[0])],
                self.dst.at[j, self.block(p.s)],
                self.ss.at[j],
                self.rs.at[j],
                peer,
            ).start()
            return carry

        lax.fori_loop(1, p.sp_count, one, 0)
        self.dst[j, self.block(p.s)] = self.src[j, self.block(p.s)]

    def all_of(self, j):
        others = pl.ds(0, (self.p.sp_count - 1) * self.rows)
        return remote(self.src.at[j, others], self.dst.at[j, others], self.ss.at[j], self.rs.at[j], self.p.peer(1))

    def wait(self, j):
        self.all_of(j).wait_recv()

    def drain(self, j):
        self.all_of(j).wait_send()


def dispatch_kernel(
    normed, pick, wg_hbm, wu_hbm, sg, su, hidden, shared,
    ring_buf, outgoing, own, other, wg, wu, gate_sum, up_sum, sgu, pre, pre_other,
    w_sem, x_send, x_recv, ring_send, ring_recv, a_send, a_recv, f_send, f_recv, s_send, s_recv,
):
    p = Place()
    c, nc = p.c, CHUNKS
    slots, rows = pick.shape
    my_rows, width = normed.shape
    half = width // 2
    fc = half // nc
    units = sg.shape[0]
    chip_rows = 2 * my_rows
    tile = min(256, slots)
    fetch_gate = pltpu.make_async_copy(wg_hbm, wg, w_sem.at[0])
    fetch_up = pltpu.make_async_copy(wu_hbm, wu, w_sem.at[1])
    fetch_gate.start()
    fetch_up.start()
    p.barrier([p.partner, p.right, p.left])

    mine = pl.ds(pl.multiple_of(p.z * chip_rows + c * my_rows, my_rows), my_rows)

    def cols(h, j):
        return pl.ds(pl.multiple_of(h * half + j * fc, fc), fc)

    def swap(j):
        return remote(normed.at[:, cols(1 - c, j)], ring_buf.at[j, mine], x_send.at[j], x_recv.at[j], p.partner)

    def swapped(j):
        theirs = pl.ds(pl.multiple_of(p.z * chip_rows + (1 - c) * my_rows, my_rows), my_rows)
        return remote(ring_buf.at[j, theirs], ring_buf.at[j, theirs], x_send.at[j], x_recv.at[j], p.partner)

    for j in range(nc):
        swap(j).start()
    half_cols = [pl.ds(pl.multiple_of(h * half, half), half) for h in (c, 1 - c)]
    sgu_rows = [pl.ds(pl.multiple_of(k * 2 * units + c * units, units), units) for k in range(2)]
    shared_swaps = [
        remote(ref.at[:, half_cols[1]], sgu.at[sgu_rows[k]], s_send.at[k], s_recv.at[k], p.partner)
        for k, ref in enumerate((sg, su))
    ]
    for copy in shared_swaps:
        copy.start()
    for k, ref in enumerate((sg, su)):
        sgu[sgu_rows[k]] = ref[:, half_cols[0]]
    for j in range(nc):
        ring_buf[j, mine] = normed[:, cols(c, j)]

    ring = RingGather(p, ring_buf, chip_rows, ring_send, ring_recv)
    spread = Exchange(p, outgoing, own, slots // p.sp_count, a_send, a_recv)
    last = p.nz // 2

    def forward(j):
        return remote(own.at[j], other.at[j], f_send.at[j], f_recv.at[j], p.partner)

    def begin(pair):
        for j in pair:
            swapped(j).wait_recv()
            ring.send(j, 1)

    def hop(pair, k):
        for j in pair:
            ring.wait(j, k)
            ring.send(j, k + 1)

    def select(j):
        ring.wait(j, last)

        def one(r):
            outgoing[j, r] = dot_nn(pick[r], ring_buf[j]).astype(jnp.bfloat16)

        rows_loop(slots, tile, one)
        spread.send(j)

    def shared_part(j):
        def one(r):
            part = dot_nt(ring_buf[j, r], sgu[:, j * fc : (j + 1) * fc])
            pre[r] = part if j == 0 else pre[r] + part

        rows_loop(rows, tile, one)

    def arrive(j):
        spread.wait(j)
        forward(j).start()

    def multiply(j):
        forward(j).wait_recv()

        def one(r):
            a, b = own[j, r], other[j, r]
            for w, total in ((wg, gate_sum), (wu, up_sum)):
                part = dot_nt(a, w[:, cols(c, j)]) + dot_nt(b, w[:, cols(1 - c, j)])
                total[r] = part if j == 0 else total[r] + part

        rows_loop(slots, tile, one)

    first, second = (0, 1), (2, 3)
    begin(first)
    for k in range(1, last):
        hop(first, k)
    begin(second)
    for j in first:
        select(j)
    for copy in shared_swaps:
        copy.wait_recv()
    for k in range(1, last):
        hop(second, k)
        if k <= 2:
            shared_part(first[k - 1])
    for j in first:
        if last <= j + 1:
            shared_part(j)
    select(2)
    arrive(0)
    select(3)
    for j in second:
        shared_part(j)
    swap_pre = remote(pre, pre_other, s_send.at[2], s_recv.at[2], p.partner)
    swap_pre.start()
    fetch_gate.wait()
    fetch_up.wait()
    multiply(0)
    arrive(1)
    swap_pre.wait_recv()

    def shared_one(r):
        both = pre[r] + pre_other[r]
        gate, up = both[:, : 2 * units], both[:, 2 * units :]
        shared[r] = (gate / (1.0 + jnp.exp(-gate)) * up).astype(jnp.bfloat16)

    rows_loop(rows, tile, shared_one)
    multiply(1)
    arrive(2)
    multiply(2)
    arrive(3)
    multiply(3)

    def hidden_one(r):
        gate = gate_sum[r]
        hidden[r] = (gate / (1.0 + jnp.exp(-gate)) * up_sum[r]).astype(jnp.bfloat16)

    rows_loop(slots, tile, hidden_one)
    for j in range(nc):
        swap(j).wait_send()
        ring.drain(j)
        spread.drain(j)
        forward(j).wait_send()
    for copy in shared_swaps:
        copy.wait_send()
    swap_pre.wait_send()


def combine_kernel(
    hidden, wd_hbm, blend, shared, sd, after_mix, out,
    wd, half_send, half_recv, total, held, sdh, part, red_send, red_recv, moe_send, moe_recv,
    w_sem, d_send, d_recv, h_send, h_recv, a_send, a_recv, r_send, r_recv, m_send, m_recv,
):
    p = Place()
    c, nc = p.c, CHUNKS
    rows, slots = blend.shape
    my_rows, width = after_mix.shape
    half = width // 2
    fc = half // nc
    units = sd.shape[0]
    chip_rows = 2 * my_rows
    tile = min(256, slots)
    fetch = pltpu.make_async_copy(wd_hbm, wd, w_sem.at[0])
    fetch.start()
    p.barrier([p.partner, p.right, p.left])

    def cols(h, j):
        return pl.ds(pl.multiple_of(h * half + j * fc, fc), fc)

    half_cols = [pl.ds(pl.multiple_of(h * half, half), half) for h in (c, 1 - c)]
    my_units = pl.ds(pl.multiple_of(c * units, units), units)
    swap_sd = remote(sd.at[:, half_cols[1]], sdh.at[my_units], d_send.at[0], d_recv.at[0], p.partner)
    swap_sd.start()
    sdh[my_units] = sd[:, half_cols[0]]
    fetch.wait()

    spread = Exchange(p, total, held, slots // p.sp_count, a_send, a_recv)

    def give(j):
        return remote(half_send.at[j], half_recv.at[j], h_send.at[j], h_recv.at[j], p.partner)

    def down(j):
        def theirs(r):
            half_send[j, r] = dot_nn(hidden[r], wd[:, cols(1 - c, j)]).astype(jnp.bfloat16)

        def ours(r):
            total[j, r] = dot_nn(hidden[r], wd[:, cols(c, j)]).astype(jnp.bfloat16)

        rows_loop(slots, tile, theirs)
        give(j).start()
        rows_loop(slots, tile, ours)

    def add_halves(j):
        give(j).wait_recv()

        def one(r):
            both = total[j, r].astype(jnp.float32) + half_recv[j, r].astype(jnp.float32)
            total[j, r] = both.astype(jnp.bfloat16)

        rows_loop(slots, tile, one)
        spread.send(j)

    def blend_rows(j):
        spread.wait(j)

        def one(r):
            mixed = dot_nn(blend[r], held[j])
            part[j, r] = mixed + dot_nn(shared[r], sdh[:, j * fc : (j + 1) * fc])

        rows_loop(rows, tile, one)

    def chip_block(distance):
        index = (p.z + distance + p.nz) % p.nz
        return pl.ds(pl.multiple_of(index * chip_rows, chip_rows), chip_rows)

    def red(j, way, m):
        return remote(
            red_send.at[j, way, m - 1],
            red_recv.at[j, way, m - 1],
            r_send.at[j, way, m - 1],
            r_recv.at[j, way, m - 1],
            p.left if way else p.right,
        )

    def step(j, m):
        for way in range(2):
            n = p.steps(j)[way]
            if m > n:
                continue
            distance = n - m + 1
            value = part[j, chip_block(-distance if way else distance)]
            if m > 1:
                red(j, way, m - 1).wait_recv()
                value = value + red_recv[j, way, m - 2].astype(jnp.float32)
            red_send[j, way, m - 1] = value.astype(jnp.bfloat16)
            red(j, way, m).start()

    def give_rows(j):
        return remote(moe_send.at[j], moe_recv.at[j], m_send.at[j], m_recv.at[j], p.partner)

    def finish(j):
        own_rows = pl.ds(pl.multiple_of(c * my_rows, my_rows), my_rows)
        their_rows = pl.ds(pl.multiple_of((1 - c) * my_rows, my_rows), my_rows)
        ends = []
        for way in range(2):
            n = p.steps(j)[way]
            if n:
                red(j, way, n).wait_recv()
                ends.append((way, n - 1))

        def moe(which, offset):
            base = pl.ds(pl.multiple_of(p.z * chip_rows + offset * my_rows, my_rows), my_rows)
            value = part[j, base]
            for way, slot in ends:
                value = value + red_recv[j, way, slot, which].astype(jnp.float32)
            return value.astype(jnp.bfloat16)

        moe_send[j] = moe(their_rows, 1 - c)
        give_rows(j).start()
        value = after_mix[:, cols(c, j)].astype(jnp.float32) + moe(own_rows, c).astype(jnp.float32)
        out[:, cols(c, j)] = value.astype(jnp.bfloat16)

    def take_rows(j):
        give_rows(j).wait_recv()
        value = after_mix[:, cols(1 - c, j)].astype(jnp.float32) + moe_recv[j].astype(jnp.float32)
        out[:, cols(1 - c, j)] = value.astype(jnp.bfloat16)

    down(0)
    for j in range(1, nc):
        down(j)
        add_halves(j - 1)
    add_halves(nc - 1)
    swap_sd.wait_recv()
    blend_rows(0)
    step(0, 1)
    step(0, 2)
    blend_rows(1)
    step(1, 1)
    step(0, 3)
    step(1, 2)
    blend_rows(2)
    step(2, 1)
    step(0, 4)
    step(1, 3)
    step(2, 2)
    blend_rows(3)
    step(3, 1)
    finish(0)
    step(1, 4)
    step(2, 3)
    step(3, 2)
    finish(1)
    step(2, 4)
    step(3, 3)
    finish(2)
    step(3, 4)
    finish(3)
    for j in range(nc):
        take_rows(j)
    swap_sd.wait_send()
    for j in range(nc):
        give(j).wait_send()
        spread.drain(j)
        give_rows(j).wait_send()
        for way in range(2):
            for m in range(1, p.steps(j)[way] + 1):
                red(j, way, m).wait_send()


def vmem():
    return pl.BlockSpec(memory_space=pltpu.VMEM)


def anywhere():
    return pl.BlockSpec(memory_space=pl.ANY)


def dispatch(normed, pick, w_gate, w_up, shared_gate, shared_up):
    nc = CHUNKS
    slots, rows = pick.shape
    width = normed.shape[1]
    half = width // 2
    fc = half // nc
    hidden_units, units = w_gate.shape[0], shared_gate.shape[0]
    hops = lax.axis_size("tp") // 4
    bf, f32 = jnp.bfloat16, jnp.float32
    dma = pltpu.SemaphoreType.DMA
    return pl.pallas_call(
        dispatch_kernel,
        name="dispatch",
        out_shape=(
            jax.ShapeDtypeStruct((slots, hidden_units), bf),
            jax.ShapeDtypeStruct((rows, 2 * units), bf),
        ),
        in_specs=[vmem(), vmem(), anywhere(), anywhere(), vmem(), vmem()],
        out_specs=(vmem(), vmem()),
        scratch_shapes=[
            pltpu.VMEM((nc, rows, fc), bf),
            pltpu.VMEM((nc, slots, fc), bf),
            pltpu.VMEM((nc, slots, fc), bf),
            pltpu.VMEM((nc, slots, fc), bf),
            pltpu.VMEM((hidden_units, width), bf),
            pltpu.VMEM((hidden_units, width), bf),
            pltpu.VMEM((slots, hidden_units), f32),
            pltpu.VMEM((slots, hidden_units), f32),
            pltpu.VMEM((4 * units, half), bf),
            pltpu.VMEM((rows, 4 * units), f32),
            pltpu.VMEM((rows, 4 * units), f32),
            dma((2,)),
            dma((nc,)),
            dma((nc,)),
            dma((nc, 2, hops)),
            dma((nc, 2, hops)),
            dma((nc,)),
            dma((nc,)),
            dma((nc,)),
            dma((nc,)),
            dma((3,)),
            dma((3,)),
        ],
        compiler_params=pltpu.CompilerParams(collective_id=1, has_side_effects=True),
    )(normed, pick, w_gate, w_up, shared_gate, shared_up)


def combine(hidden, w_down, blend, shared, shared_down, after_mix):
    nc = CHUNKS
    rows, slots = blend.shape
    my_rows, width = after_mix.shape
    half = width // 2
    fc = half // nc
    hidden_units, units = w_down.shape[0], shared_down.shape[0]
    hops = lax.axis_size("tp") // 4
    bf, f32 = jnp.bfloat16, jnp.float32
    dma = pltpu.SemaphoreType.DMA
    return pl.pallas_call(
        combine_kernel,
        name="combine",
        out_shape=jax.ShapeDtypeStruct((my_rows, width), bf),
        in_specs=[vmem(), anywhere(), vmem(), vmem(), vmem(), vmem()],
        out_specs=vmem(),
        scratch_shapes=[
            pltpu.VMEM((hidden_units, width), bf),
            pltpu.VMEM((nc, slots, fc), bf),
            pltpu.VMEM((nc, slots, fc), bf),
            pltpu.VMEM((nc, slots, fc), bf),
            pltpu.VMEM((nc, slots, fc), bf),
            pltpu.VMEM((2 * units, half), bf),
            pltpu.VMEM((nc, rows, fc), f32),
            pltpu.VMEM((nc, 2, hops, 2 * my_rows, fc), bf),
            pltpu.VMEM((nc, 2, hops, 2 * my_rows, fc), bf),
            pltpu.VMEM((nc, my_rows, fc), bf),
            pltpu.VMEM((nc, my_rows, fc), bf),
            dma((1,)),
            dma((1,)),
            dma((1,)),
            dma((nc,)),
            dma((nc,)),
            dma((nc,)),
            dma((nc,)),
            dma((nc, 2, hops)),
            dma((nc, 2, hops)),
            dma((nc,)),
            dma((nc,)),
        ],
        compiler_params=pltpu.CompilerParams(collective_id=2, has_side_effects=True),
    )(hidden, w_down, blend, shared, shared_down, after_mix)


def slot_matrices(ids, weights, experts, capacity, lanes, lane):
    rows = ids.shape[0]
    slots = experts // lanes * capacity
    named = ids[:, :, None] == jnp.arange(experts, dtype=jnp.int32)
    weight = jnp.sum(jnp.where(named, weights[:, :, None], 0.0), axis=1)
    named = jnp.any(named, axis=1)
    index = jnp.arange(rows, dtype=jnp.int32)
    before = (index[None, :] < index[:, None]).astype(jnp.bfloat16)
    rank = dot_nn(before, named.astype(jnp.bfloat16))
    rank = jnp.where(named, rank, -1.0).astype(jnp.bfloat16)
    slot = jnp.arange(slots, dtype=jnp.int32)
    holds = slot[:, None] // capacity * lanes + lane == jnp.arange(experts, dtype=jnp.int32)
    holds = holds.astype(jnp.bfloat16)
    place = (slot % capacity).astype(jnp.float32)
    pick = (dot_nt(holds, rank) == place[:, None]).astype(jnp.bfloat16)
    blend = jnp.where(
        dot_nt(rank, holds) == place[None, :], dot_nt(weight.astype(jnp.bfloat16), holds), 0.0
    )
    return pick, blend.astype(jnp.bfloat16)


def body(
    queries,
    keys,
    values,
    sink_logits,
    w_out,
    residual,
    norm_gain,
    expert_ids,
    expert_weights,
    w_gate,
    w_up,
    w_down,
    shared_gate,
    shared_up,
    shared_down,
):
    tp_count = lax.axis_size("tp")
    sp_count = lax.axis_size("sp")
    seq_rows = queries.shape[0]
    expert_count = sp_count * tp_count // 2
    capacity = CAP
    local_heads = queries.shape[1] // HD
    kv_start = lax.axis_index("tp") * local_heads // GROUP * HD
    key_cols = lax.dynamic_slice_in_dim(keys, kv_start, HD, 1)
    value_cols = lax.dynamic_slice_in_dim(values, kv_start, HD, 1)
    rim_keys, rim_values = shifted(
        (key_cols[seq_rows - WINDOW :], value_cols[seq_rows - WINDOW :]), "sp", 1
    )
    num_blocks = seq_rows // WINDOW
    key_blocks = key_cols.reshape(num_blocks, WINDOW, HD)
    value_blocks = value_cols.reshape(num_blocks, WINDOW, HD)
    keys_ext = jnp.concatenate(
        [jnp.concatenate([rim_keys[None], key_blocks[:-1]], axis=0), key_blocks], axis=1
    )
    values_ext = jnp.concatenate(
        [jnp.concatenate([rim_values[None], value_blocks[:-1]], axis=0), value_blocks], axis=1
    )
    query_blocks = queries.reshape(num_blocks, WINDOW, local_heads, HD)
    scores = jnp.einsum(
        "nqhd,nsd->nhqs", query_blocks, keys_ext, preferred_element_type=jnp.float32
    ) * HD ** (-0.5)
    query_pos = jnp.arange(WINDOW)[:, None] + WINDOW
    key_pos = jnp.arange(2 * WINDOW)[None, :]
    in_band = (key_pos <= query_pos) & (key_pos > query_pos - WINDOW)
    absolute = (
        lax.axis_index("sp") * seq_rows
        + jnp.arange(num_blocks)[:, None, None] * WINDOW
        + key_pos[None]
        - WINDOW
    )
    allowed = in_band[None] & (absolute >= 0)
    scores = jnp.where(allowed[:, None], scores, -jnp.inf)
    sink_col = jnp.broadcast_to(sink_logits[None, :, None, None], scores.shape[:-1] + (1,))
    combined = jnp.concatenate([scores, sink_col], axis=-1)
    row_max = jnp.max(combined, axis=-1, keepdims=True)
    exps = jnp.exp(combined - row_max)
    weights = (exps[..., :-1] / jnp.sum(exps, axis=-1, keepdims=True)).astype(jnp.bfloat16)
    attended = jnp.einsum("nhqs,nsd->nqhd", weights, values_ext, preferred_element_type=jnp.float32)
    attended = attended.astype(jnp.bfloat16).reshape(seq_rows, local_heads * HD)
    head_rows = lax.all_to_all(attended, "tp", split_axis=0, concat_axis=1, tiled=True)
    projected = jnp.dot(
        head_rows,
        lax.all_gather(w_out, "tp", axis=0, tiled=True),
        preferred_element_type=jnp.float32,
    )
    after_mix = (residual.astype(jnp.float32) + projected).astype(jnp.bfloat16)
    normed = normalize(after_mix, norm_gain)
    lanes = tp_count // 2
    pick, blend = slot_matrices(
        expert_ids, expert_weights, expert_count, capacity, lanes, lax.axis_index("tp") // 2
    )
    hidden, shared = dispatch(normed, pick, w_gate[0], w_up[0], shared_gate, shared_up)
    return combine(hidden, w_down[0], blend, shared, shared_down, after_mix)


def solution(mesh):
    return jax.shard_map(
        body,
        mesh=mesh,
        in_specs=(
            P("sp", "tp"),
            P("sp", None),
            P("sp", None),
            P("tp"),
            P("tp", None),
            P(("sp", "tp"), None),
            P(),
            P("sp", None),
            P("sp", None),
            P(("sp", "tp"), None, None),
            P(("sp", "tp"), None, None),
            P(("sp", "tp"), None, None),
            P("tp", None),
            P("tp", None),
            P("tp", None),
        ),
        out_specs=P(("sp", "tp"), None),
        check_vma=False,
    )
```

time: 362 us -> 186 us (0.51)
  waiting for transfers between devices: 173 us -> 20.8 us
  Pallas kernels: 0 us -> 116 us
  local copies, waits for them, and re-layouts: 73.6 us -> 4.7 us
  matrix products: 38.2 us -> 9.73 us
  blocking collectives: 19.9 us -> 0 us
  other arithmetic: 20 us -> 3.55 us
    pallas_call x0 -> x2, Pallas kernels: none -> 116 us  [the longest x1 63 us: dispatch(): pl.pallas_call(dispatch_kernel, name='dispatch', out_shape=(jax.ShapeDtyp...]
    all_to_all x2 -> x1, waiting for transfers between devices: 85 us -> 8.4 us  [body(): lax.all_to_all(attended, 'tp', split_axis=0, concat_axis=1, tiled=True)]
    reduce_scatter x1 -> x0, waiting for transfers between devices: 56.6 us -> none  [body(): lax.psum_scatter(partial_sum.astype(jnp.bfloat16), 'tp', scatter_dimensio...]
    gather x5 -> x0, local copies, waits for them, and re-layouts: 35.7 us -> none  [the longest x4 24.1 us: body(): held[position[:, route_slot]].astype(jnp.float32)]
    dot_general x4, matrix products: 33.3 us -> 5.79 us  [the longest x3 5.06 us: dot_nt(): lax.dot_general(a, b, (((1,), (1,)), ((), ())), preferred_element_type=jn...]
    all_to_all x1 -> x0, blocking collectives: 19.9 us -> none  [body(): lax.all_to_all(attended, 'tp', split_axis=0, concat_axis=1, tiled=True)]
    scatter x1 -> x0, local copies, waits for them, and re-layouts: 15.5 us -> none  [slot_layout(): jnp.full((expert_count * capacity,), -1, jnp.int32).at[slot_index]]
    all_gather x1 -> x0, waiting for transfers between devices: 12.3 us -> none  [body(): all_rows = lax.all_gather(normed, 'tp', axis=0, tiled=True)]
  transfers between devices with their start and end apart: 8 -> 4, of which waited for: 6 -> 2; matrix products, arithmetic and copies ran while one was open for 12% -> 7% of each run, Pallas kernels for 0% -> 0%
where the time goes in v1:
time: 186 us
  Pallas kernels  116 us (62%)
  waiting for transfers between devices  20.8 us (11%)
  starting transfers between devices  16.8 us (9%)
  between operations  14.4 us (8%)
  matrix products  9.73 us (5%)
  local copies, waits for them, and re-layouts  4.7 us (3%)
  other arithmetic  3.55 us (2%)
    pallas_call x1, Pallas kernels, dispatch(): pl.pallas_call(dispatch_kernel, name='dispatch', out_shape=(jax.ShapeDtyp...  63 us
    pallas_call x1, Pallas kernels, combine(): pl.pallas_call(combine_kernel, name='combine', out_shape=jax.ShapeDtypeSt...  53 us
    all_gather x1, waiting for transfers between devices, body(): lax.all_gather(w_out, 'tp', axis=0, tiled=True)  11.7 us
    all_to_all x1, starting transfers between devices, body(): lax.all_to_all(attended, 'tp', split_axis=0, concat_axis=1, tiled=True)  9.71 us
    all_to_all x1, waiting for transfers between devices, body(): lax.all_to_all(attended, 'tp', split_axis=0, concat_axis=1, tiled=True)  8.4 us
    ppermute x2, starting transfers between devices, shifted(): return lax.ppermute(block, axis, route)  7.05 us
    dot_general x3, matrix products, dot_nt(): lax.dot_general(a, b, (((1,), (1,)), ((), ())), preferred_element_type=jn...  5.06 us
  transfers between devices with their start and end apart: 4, of which 2 were waited for; matrix products, arithmetic and copies ran while one was open for 7% of the time, Pallas kernels for 0%

profile of v1, /device:TPU:1, one launch (start us, length us, event | category | flops | bytes accessed | tf_op | source)
XLA Modules:
  0.0 186.0 jit_solution(7991205562474758658)
XLA Ops:
  6.5 0.0 copy-start
  6.5 0.0 copy-start.3
  6.5 0.0 copy-start.4
  6.5 0.0 all-gather.2.cloned.1.call-start
  6.5 0.7 all-gather.2.cloned.1.call-update
  7.3 1.2 constant_dynamic-slice_fusion
  8.5 0.1 copy.61
  8.7 3.9 %collective-permute-start.1 = (bf16[128,64]{0,1:T(8,128)(2,1)S(1)}, bf16[128,64]{0,1:T(8,128)(2,1)S(1)}, u32[]{:S(2)}, u32[]{:S(2)}) collective-permute-start(bf16[128,64]{0,1:T(8,128)(2,1)S(1)} %slice.30), channel_id=1, source_target_pairs={{0,16},{16,32},{32,48},{48,64},{64,80},{80,96},{96,112},{112,128},... | collective-permute-start | bytes 49160 | tf_op jit(solution)/shard_map/ppermute | solution.py:17
  12.6 0.1 copy.60
  12.8 3.1 %collective-permute-start = (bf16[128,64]{0,1:T(8,128)(2,1)S(1)}, bf16[128,64]{0,1:T(8,128)(2,1)S(1)}, u32[]{:S(2)}, u32[]{:S(2)}) collective-permute-start(bf16[128,64]{0,1:T(8,128)(2,1)S(1)} %slice.28), channel_id=1, source_target_pairs={{0,16},{16,32},{32,48},{48,64},{64,80},{80,96},{96,112},{112,128},... | collective-permute-start | bytes 49160 | tf_op jit(solution)/shard_map/ppermute | solution.py:17
  16.0 0.0 copy-done.3
  16.0 0.9 fusion.2
  16.9 0.0 copy-done.4
  16.9 1.4 select_reduce_fusion
  18.5 0.7 fusion.6
  19.2 0.8 fusion.13
  20.1 2.1 %select_convert_fusion.blend = bf16[1024,1024]{1,0:T(8,128)(2,1)} fusion(f32[1024,1024]{1,0:T(8,128)S(1)} %fusion.13, f32[1024]{0:T(1024)S(1)} %get-tuple-element.16, bf16[1024,128]{1,0:T(8,128)(2,1)S(1)} %select_reduce_fusion, s32[1024]{0:T(1024)S(1)} %get-tuple-element.15), kind=kOutput, calls=%fused_computation | convolution fusion | flops 271712256 | bytes 6561792 | tf_op jit(solution)/shard_map/dot_general | solution.py:32
  22.2 0.1 add_compare_fusion
  22.9 0.0 collective-permute-done.1
  22.9 0.0 copy-done
  23.0 0.5 fusion.5
  23.5 0.1 pad_reduce_fusion
  23.6 0.2 fusion.44
  23.7 0.0 collective-permute-done
  23.7 0.2 fusion.7
  24.0 0.1 copy.55
  24.1 0.0 copy-start.2
  24.1 0.1 all_to_all.14
  24.2 0.1 copy.76
  24.3 0.9 reshape.199
  25.2 9.7 %all-to-all-start = ((bf16[16,2,2048]{2,1,0:T(2,128)(2,1)}), bf16[16,2,2048]{2,1,0:T(2,128)(2,1)S(1)}, u32[]{:S(2)}, u32[]{:S(2)}) async-start(bf16[16,2,2048]{2,1,0:T(2,128)(2,1)} %reshape.199), calls=%async_computation | async-start | bytes 262144 | tf_op jit(solution)/shard_map/all_to_all | solution.py:644
  34.9 2.1 %compare_convert_fusion.pick = bf16[1024,1024]{1,0:T(8,128)(2,1)} fusion(f32[1024]{0:T(1024)S(1)} %get-tuple-element.16, bf16[1024,128]{1,0:T(8,128)(2,1)S(1)} %fusion.6, s32[1024]{0:T(1024)S(1)} %get-tuple-element.15), kind=kOutput, calls=%fused_computation.2 | convolution fusion | flops 270663680 | bytes 2367488 | tf_op jit(solution)/shard_map/dot_general | solution.py:32
  37.0 8.4 %all-to-all-done = bf16[16,2,2048]{2,1,0:T(2,128)(2,1)S(1)} async-done(((bf16[16,2,2048]{2,1,0:T(2,128)(2,1)}), bf16[16,2,2048]{2,1,0:T(2,128)(2,1)S(1)}, u32[]{:S(2)}, u32[]{:S(2)}) %all-to-all-start) | async-done | bytes 131104 | tf_op jit(solution)/shard_map/all_to_all | solution.py:644
  45.4 0.2 reshape.200
  45.6 11.7 %all-gather.2.cloned.1.call-done = bf16[1024,2048]{1,0:T(8,128)(2,1)} async-done(((bf16[64,2048]{1,0:T(8,128)(2,1)}), bf16[1024,2048]{1,0:T(8,128)(2,1)}) %all-gather.2.cloned.1.call-update) | async-done | bytes 4194320 | tf_op jit(solution)/shard_map/all_gather | solution.py:647
  57.4 0.0 copy-done.2
  57.4 0.0 copy-start.5
  57.4 3.2 %fusion.9 = (f32[64]{0:T(128)S(1)}, bf16[64,2048]{1,0:T(8,128)(2,1)S(1)}) fusion(bf16[64,1024]{0,1:T(8,128)(2,1)S(1)} %bitcast.68, bf16[1024,2048]{1,0:T(8,128)(2,1)} %all-gather.2.cloned.1.call-done, bf16[64,2048]{1,0:T(8,128)(2,1)S(1)} %copy-done.2), kind=kOutput, calls=%fused_computation.22 | convolution fusion | flops 269221824 | bytes 4849920 | tf_op jit(solution)/shard_map/dot_general | solution.py:645
  60.6 0.0 copy-start.1
  60.6 0.0 copy-done.5
  60.6 0.8 fusion.11.normed
  61.4 63.0 %dispatch.1 = (bf16[1024,768]{1,0:T(8,128)(2,1)}, bf16[1024,64]{1,0:T(8,128)(2,1)}) custom-call(bf16[64,2048]{1,0:T(8,128)(2,1)} %fusion.11.normed, bf16[1024,1024]{1,0:T(8,128)(2,1)} %compare_convert_fusion.pick, bf16[768,2048]{1,0:T(8,128)(2,1)} %bitcast.65, bf16[768,2048]{1,0:T(8,128)(2,1)} %bitcast.66, bf16[32,2048]{1,0:T(8,128)(2,1)} %sg.1, ...), custom_call_target="tpu_custom_call" | custom-call | tf_op jit(solution)/shard_map/dispatch/pallas_call | solution.py:482
  124.5 0.0 copy-done.1
  124.5 53.0 %combine.1 = bf16[64,2048]{1,0:T(8,128)(2,1)} custom-call(bf16[1024,768]{1,0:T(8,128)(2,1)} %get-tuple-element.7.hidden, bf16[768,2048]{1,0:T(8,128)(2,1)} %bitcast.67, bf16[1024,1024]{1,0:T(8,128)(2,1)} %select_convert_fusion.blend, bf16[1024,64]{1,0:T(8,128)(2,1)} %get-tuple-element.8.shared, bf16[32,2048]{1,0:T(8,128)(2,1)} %sd.1, bf16[64,2048]{1,0:T(8,128)(2,1)} %copy-done.1), custom_call_target="tpu_custom_call" | custom-call | tf_op jit(solution)/shard_map/combine/pallas_call | solution.py:529
  177.5 1.7 copy.79
  (11 shorter events, 0.2 us)
Async XLA Ops:
  6.5 16.4 %copy-start = (bf16[1024,64]{0,1:T(8,128)(2,1)S(1)}, bf16[1024,64]{0,1:T(8,128)(2,1)}, u32[]{:S(2)}) copy-start(bf16[1024,64]{0,1:T(8,128)(2,1)} %param.15) | copy-start | bytes 393220
  6.5 9.4 %copy-start.3 = (s32[1024,4]{0,1:T(4,128)S(1)}, s32[1024,4]{0,1:T(4,128)}, u32[]{:S(2)}) copy-start(s32[1024,4]{0,1:T(4,128)} %param.22) | copy-start | bytes 49156
  6.5 10.4 %copy-start.4 = (f32[1024,4]{0,1:T(4,128)S(1)}, f32[1024,4]{0,1:T(4,128)}, u32[]{:S(2)}) copy-start(f32[1024,4]{0,1:T(4,128)} %param.23) | copy-start | bytes 49156
  6.5 50.8 %all-gather.2.cloned.1.call-start = ((), (), s32[]{:S(2)}) async-start(), calls=%async_computation.1 | async-start | bytes 4456448 | tf_op jit(solution)/shard_map/all_gather | solution.py:647
  8.7 14.3 %collective-permute-start.1 = (bf16[128,64]{0,1:T(8,128)(2,1)S(1)}, bf16[128,64]{0,1:T(8,128)(2,1)S(1)}, u32[]{:S(2)}, u32[]{:S(2)}) collective-permute-start(bf16[128,64]{0,1:T(8,128)(2,1)S(1)} %slice.30), channel_id=1, source_target_pairs={{0,16},{16,32},{32,48},{48,64},{64,80},{80,96},{96,112},{112,128},... | collective-permute-start | bytes 49160 | tf_op jit(solution)/shard_map/ppermute | solution.py:17
  12.8 11.0 %collective-permute-start = (bf16[128,64]{0,1:T(8,128)(2,1)S(1)}, bf16[128,64]{0,1:T(8,128)(2,1)S(1)}, u32[]{:S(2)}, u32[]{:S(2)}) collective-permute-start(bf16[128,64]{0,1:T(8,128)(2,1)S(1)} %slice.28), channel_id=1, source_target_pairs={{0,16},{16,32},{32,48},{48,64},{64,80},{80,96},{96,112},{112,128},... | collective-permute-start | bytes 49160 | tf_op jit(solution)/shard_map/ppermute | solution.py:17
  24.1 33.3 %copy-start.2 = (bf16[64,2048]{1,0:T(8,128)(2,1)S(1)}, bf16[64,2048]{1,0:T(8,128)(2,1)}, u32[]{:S(2)}) copy-start(bf16[64,2048]{1,0:T(8,128)(2,1)} %param.20) | copy-start | bytes 786436
  25.2 20.2 %all-to-all-start = ((bf16[16,2,2048]{2,1,0:T(2,128)(2,1)}), bf16[16,2,2048]{2,1,0:T(2,128)(2,1)S(1)}, u32[]{:S(2)}, u32[]{:S(2)}) async-start(bf16[16,2,2048]{2,1,0:T(2,128)(2,1)} %reshape.199), calls=%async_computation | async-start | bytes 262144 | tf_op jit(solution)/shard_map/all_to_all | solution.py:644
  57.4 3.2 %copy-start.5 = (f32[2048]{0:T(1024)S(1)}, f32[2048]{0:T(1024)}, u32[]{:S(2)}) copy-start(f32[2048]{0:T(1024)} %param.21) | copy-start | bytes 24580
  60.6 63.9 %copy-start.1 = (bf16[64,2048]{1,0:T(8,128)(2,1)}, bf16[64,2048]{1,0:T(8,128)(2,1)S(1)}, u32[]{:S(2)}) copy-start(bf16[64,2048]{1,0:T(8,128)(2,1)S(1)} %get-tuple-element.12.after_mix) | copy-start | bytes 786436
Sparse Core Ops, SparseCore 0:
  9.2 48.1 all-gather.1

commit v2 on v1

--- a/solution.py
+++ b/solution.py
@@ -9,18 +9,6 @@
 GROUP = 4
 WINDOW = 128
 TOPK = 4
-
-
-def shifted(block, axis, distance):
-    devices = range(lax.axis_size(axis))
-    route = [(i - distance, i) for i in devices if i - distance in devices]
-    return lax.ppermute(block, axis, route)
-
-
-def normalize(after_mix, norm_gain):
-    values_f = after_mix.astype(jnp.float32)
-    scale = lax.rsqrt(jnp.mean(values_f * values_f, axis=-1, keepdims=True) + 1e-06)
-    return (values_f * scale * norm_gain).astype(jnp.bfloat16)
 
 
 MESH = pl.DeviceIdType.MESH
@@ -149,19 +137,255 @@
         self.all_of(j).wait_send()
 
 
+def mix_kernel(
+    queries, keys, values, sink, w_out, residual, gain, ids, weights,
+    normed, after, pick, blend,
+    key_ext, value_ext, att, heads, heads_t, wide, res, square, square_other,
+    rank_buf, weight_buf,
+    k_send, k_recv, h_send, h_recv, x_send, x_recv, ring_send, ring_recv, r_send, r_recv, q_send, q_recv,
+):
+    p = Place()
+    c, nc = p.c, CHUNKS
+    rows = queries.shape[0]
+    my_rows, width = residual.shape
+    half = width // 2
+    fc = half // nc
+    head_rows = w_out.shape[0]
+    chip_rows = 2 * my_rows
+    blocks = rows // WINDOW
+    experts = p.sp_count * p.nz
+    kv = p.t // GROUP
+    kv_cols = pl.ds(pl.multiple_of(kv // 2 * 128, 128), 128)
+    f32, bf = jnp.float32, jnp.bfloat16
+
+    sem = pltpu.get_barrier_semaphore()
+
+    def greet(o, carry):
+        pl.semaphore_signal(
+            sem, inc=1, device_id=(p.s, (p.t + o) % p.tp_count), device_id_type=MESH
+        )
+        return carry
+
+    lax.fori_loop(1, p.tp_count, greet, 0)
+    following = ((p.s + 1) % p.sp_count, p.t)
+    for device in (following, ((p.s + p.sp_count - 1) % p.sp_count, p.t)):
+        pl.semaphore_signal(sem, inc=1, device_id=device, device_id_type=MESH)
+    pl.semaphore_wait(sem, p.tp_count + 1)
+
+    rim = pl.ds(rows - WINDOW, WINDOW)
+    halo = [
+        remote(ref.at[rim, kv_cols], ext.at[pl.ds(0, WINDOW)], k_send.at[i], k_recv.at[i], following)
+        for i, (ref, ext) in enumerate(((keys, key_ext), (values, value_ext)))
+    ]
+
+    def half_of(h):
+        return pl.ds(pl.multiple_of(h * half, half), half)
+
+    def cols(h, j):
+        return pl.ds(pl.multiple_of(h * half + j * fc, fc), fc)
+
+    def shard(core):
+        return pl.ds(pl.multiple_of(p.z * 2 * head_rows + core * head_rows, head_rows), head_rows)
+
+    def swap(j, core):
+        return remote(
+            w_out.at[:, cols(1 - c, j)], wide.at[j, shard(core)], x_send.at[j], x_recv.at[j], p.partner
+        )
+
+    my_part = pl.ds(pl.multiple_of(c * my_rows, my_rows), my_rows)
+    swap_res = remote(residual.at[:, half_of(1 - c)], res.at[my_part], r_send.at[0], r_recv.at[0], p.partner)
+    for j in range(nc):
+        swap(j, c).start()
+    sends_rim, gets_rim = p.s + 1 < p.sp_count, p.s > 0
+
+    @pl.when(sends_rim)
+    def _():
+        for copy in halo:
+            copy.start()
+
+    swap_res.start()
+    for j in range(nc):
+        wide[j, shard(c)] = w_out[:, cols(c, j)]
+    res[my_part] = residual[:, half_of(c)]
+    ring = RingGather(p, wide, 2 * head_rows, ring_send, ring_recv)
+    last = p.nz // 2
+    everything = tuple(range(nc))
+    for j in everything:
+        swap(j, 1 - c).wait_recv()
+        ring.send(j, 1)
+
+    def hop(k):
+        for j in everything:
+            ring.wait(j, k)
+            ring.send(j, k + 1)
+
+    key_ext[pl.ds(WINDOW, rows)] = keys[:, kv_cols]
+    value_ext[pl.ds(WINDOW, rows)] = values[:, kv_cols]
+
+    @pl.when(jnp.logical_not(gets_rim))
+    def _():
+        key_ext[pl.ds(0, WINDOW)] = jnp.zeros((WINDOW, 128), bf)
+        value_ext[pl.ds(0, WINDOW)] = jnp.zeros((WINDOW, 128), bf)
+
+    tile = min(256, rows)
+    capacity = pick.shape[0] // p.sp_count
+    slots = pick.shape[0]
+    shift = capacity.bit_length() - 1
+
+    def iota(shape, axis):
+        return lax.broadcasted_iota(jnp.int32, shape, axis)
+
+    def name_rows(r):
+        lanes = iota((tile, experts), 1)
+        named = jnp.zeros((tile, experts), f32)
+        weight = jnp.zeros((tile, experts), f32)
+        tile_ids, tile_weights = ids[r], weights[r]
+        for k in range(TOPK):
+            same = tile_ids[:, k : k + 1] == lanes
+            named = jnp.where(same, 1.0, named)
+            weight = jnp.where(same, tile_weights[:, k : k + 1], weight)
+        rank_buf[r] = named.astype(bf)
+        weight_buf[r] = weight.astype(bf)
+
+    rows_loop(rows, tile, name_rows)
+    all_named = rank_buf[...]
+    ranks = []
+    for i in range(rows // tile):
+        before = iota((tile, rows), 1) < iota((tile, rows), 0) + i * tile
+        rank = dot_nn(jnp.where(before, 1.0, 0.0).astype(bf), all_named)
+        named = all_named[i * tile : (i + 1) * tile].astype(f32) > 0.0
+        ranks.append(jnp.where(named, rank, -1.0).astype(bf))
+    for i, rank in enumerate(ranks):
+        rank_buf[pl.ds(i * tile, tile)] = rank
+
+    def holds(first, count):
+        slot = iota((count, experts), 0) + first
+        same = jnp.right_shift(slot, shift) * p.nz + p.z == iota((count, experts), 1)
+        return jnp.where(same, 1.0, 0.0).astype(bf)
+
+    def fill_pick(i, carry):
+        first = i * tile
+        place = jnp.bitwise_and(iota((tile, rows), 0) + first, capacity - 1).astype(f32)
+        hit = dot_nt(holds(first, tile), rank_buf[...]) == place
+        pick[pl.ds(pl.multiple_of(first, tile), tile)] = jnp.where(hit, 1.0, 0.0).astype(bf)
+        return carry
+
+    lax.fori_loop(0, slots // tile, fill_pick, 0)
+    all_holds = holds(0, slots)
+
+    def fill_blend(r):
+        place = jnp.bitwise_and(iota((tile, slots), 1), capacity - 1).astype(f32)
+        hit = dot_nt(rank_buf[r], all_holds) == place
+        blend[r] = jnp.where(hit, dot_nt(weight_buf[r], all_holds), 0.0).astype(bf)
+
+    @pl.when(gets_rim)
+    def _():
+        for copy in halo:
+            copy.wait_recv()
+
+    lane_half = kv % 2
+    sink_value = sink[...]
+
+    def attend(i, carry):
+        b = (p.z + i) % blocks
+        ext = pl.ds(pl.multiple_of(b * WINDOW, WINDOW), 2 * WINDOW)
+        query = queries[pl.ds(pl.multiple_of(b * WINDOW, WINDOW), WINDOW)]
+        query = jnp.concatenate([query, query], axis=1)
+        in_half = jnp.right_shift(iota((WINDOW, 2 * HD), 1), HD.bit_length() - 1) == lane_half
+        query = jnp.where(in_half, query.astype(f32), 0.0).astype(bf)
+        scores = dot_nt(key_ext[ext], query) * HD ** (-0.5)
+        key_pos = iota((2 * WINDOW, WINDOW), 0)
+        query_pos = iota((2 * WINDOW, WINDOW), 1) + WINDOW
+        first_key = jnp.where(p.s * blocks + b == 0, WINDOW, 0)
+        allowed = (key_pos <= query_pos) & (key_pos > query_pos - WINDOW) & (key_pos >= first_key)
+        scores = jnp.where(allowed, scores, -jnp.inf)
+        top = jnp.maximum(jnp.max(scores, axis=0, keepdims=True), sink_value)
+        exps = jnp.exp(scores - top)
+        total = jnp.sum(exps, axis=0, keepdims=True) + jnp.exp(sink_value - top)
+        shares = (exps / total).astype(bf)
+        both = lax.dot_general(
+            value_ext[ext], shares, (((0,), (0,)), ((), ())), preferred_element_type=f32
+        )
+        att[b] = jnp.where(lane_half == 0, both[:HD], both[HD:]).astype(bf)
+        for core in range(2):
+            target = 2 * b + core
+
+            @pl.when(target != p.t)
+            def _():
+                head_piece(b, (p.s, target)).start()
+
+            @pl.when(target == p.t)
+            def _():
+                heads[head_place] = att[b]
+
+        return carry
+
+    head_place = pl.ds(pl.multiple_of(p.t * HD, HD), HD)
+
+    def head_piece(b, device):
+        return remote(att.at[b], heads.at[head_place], h_send.at[0], h_recv.at[0], device)
+
+    others = heads.at[pl.ds(0, (p.tp_count - 1) * HD)]
+    head_total = remote(others, others, h_send.at[0], h_recv.at[0], p.partner)
+
+    lax.fori_loop(0, blocks // 2, attend, 0)
+    for k in range(1, last):
+        hop(k)
+        if k == 1:
+            lax.fori_loop(blocks // 2, blocks, attend, 0)
+        if k == min(2, last - 1):
+            rows_loop(rows, tile, fill_blend)
+    head_total.wait_recv()
+    heads_t[...] = heads[...].T
+    swap_res_in = remote(
+        residual.at[:, half_of(1 - c)],
+        res.at[pl.ds(pl.multiple_of((1 - c) * my_rows, my_rows), my_rows)],
+        r_send.at[0], r_recv.at[0], p.partner,
+    )
+    swap_res_in.wait_recv()
+    squares = jnp.zeros((chip_rows, 1), f32)
+    for j in range(nc):
+        ring.wait(j, last)
+        piece = pl.ds(j * fc, fc)
+        mixed = res[:, piece].astype(f32) + dot_nn(heads_t[...], wide[j])
+        mixed = mixed.astype(bf)
+        after[:, piece] = mixed
+        mixed = mixed.astype(f32)
+        squares = squares + jnp.sum(mixed * mixed, axis=1, keepdims=True)
+    square[...] = jnp.broadcast_to(squares, square.shape)
+    swap_square = remote(square, square_other, q_send.at[0], q_recv.at[0], p.partner)
+    swap_square.start()
+    swap_square.wait_recv()
+    mean = (square[...] + square_other[...])[:, :1] / width
+    scale = lax.rsqrt(mean + 1e-06)
+    for j in range(nc):
+        piece = pl.ds(j * fc, fc)
+        normed[:, piece] = (after[:, piece].astype(f32) * scale * gain[:, cols(c, j)]).astype(bf)
+
+    @pl.when(sends_rim)
+    def _():
+        for copy in halo:
+            copy.wait_send()
+
+    for j in range(nc):
+        swap(j, c).wait_send()
+        ring.drain(j)
+    swap_res.wait_send()
+    head_total.wait_send()
+    swap_square.wait_send()
+
+
 def dispatch_kernel(
     normed, pick, wg_hbm, wu_hbm, sg, su, hidden, shared,
     ring_buf, outgoing, own, other, wg, wu, gate_sum, up_sum, sgu, pre, pre_other,
-    w_sem, x_send, x_recv, ring_send, ring_recv, a_send, a_recv, f_send, f_recv, s_send, s_recv,
+    w_sem, ring_send, ring_recv, a_send, a_recv, f_send, f_recv, s_send, s_recv,
 ):
     p = Place()
     c, nc = p.c, CHUNKS
     slots, rows = pick.shape
-    my_rows, width = normed.shape
-    half = width // 2
+    chip_rows, half = normed.shape
     fc = half // nc
     units = sg.shape[0]
-    chip_rows = 2 * my_rows
     tile = min(256, slots)
     fetch_gate = pltpu.make_async_copy(wg_hbm, wg, w_sem.at[0])
     fetch_up = pltpu.make_async_copy(wu_hbm, wu, w_sem.at[1])
@@ -169,20 +393,11 @@
     fetch_up.start()
     p.barrier([p.partner, p.right, p.left])
 
-    mine = pl.ds(pl.multiple_of(p.z * chip_rows + c * my_rows, my_rows), my_rows)
+    mine = pl.ds(pl.multiple_of(p.z * chip_rows, chip_rows), chip_rows)
 
     def cols(h, j):
         return pl.ds(pl.multiple_of(h * half + j * fc, fc), fc)
 
-    def swap(j):
-        return remote(normed.at[:, cols(1 - c, j)], ring_buf.at[j, mine], x_send.at[j], x_recv.at[j], p.partner)
-
-    def swapped(j):
-        theirs = pl.ds(pl.multiple_of(p.z * chip_rows + (1 - c) * my_rows, my_rows), my_rows)
-        return remote(ring_buf.at[j, theirs], ring_buf.at[j, theirs], x_send.at[j], x_recv.at[j], p.partner)
-
-    for j in range(nc):
-        swap(j).start()
     half_cols = [pl.ds(pl.multiple_of(h * half, half), half) for h in (c, 1 - c)]
     sgu_rows = [pl.ds(pl.multiple_of(k * 2 * units + c * units, units), units) for k in range(2)]
     shared_swaps = [
@@ -194,7 +409,7 @@
     for k, ref in enumerate((sg, su)):
         sgu[sgu_rows[k]] = ref[:, half_cols[0]]
     for j in range(nc):
-        ring_buf[j, mine] = normed[:, cols(c, j)]
+        ring_buf[j, mine] = normed[:, j * fc : (j + 1) * fc]
 
     ring = RingGather(p, ring_buf, chip_rows, ring_send, ring_recv)
     spread = Exchange(p, outgoing, own, slots // p.sp_count, a_send, a_recv)
@@ -205,7 +420,6 @@
 
     def begin(pair):
         for j in pair:
-            swapped(j).wait_recv()
             ring.send(j, 1)
 
     def hop(pair, k):
@@ -291,7 +505,6 @@
 
     rows_loop(slots, tile, hidden_one)
     for j in range(nc):
-        swap(j).wait_send()
         ring.drain(j)
         spread.drain(j)
         forward(j).wait_send()
@@ -308,11 +521,10 @@
     p = Place()
     c, nc = p.c, CHUNKS
     rows, slots = blend.shape
-    my_rows, width = after_mix.shape
-    half = width // 2
+    chip_rows, half = after_mix.shape
+    my_rows = chip_rows // 2
     fc = half // nc
     units = sd.shape[0]
-    chip_rows = 2 * my_rows
     tile = min(256, slots)
     fetch = pltpu.make_async_copy(wd_hbm, wd, w_sem.at[0])
     fetch.start()
@@ -402,22 +614,22 @@
                 red(j, way, n).wait_recv()
                 ends.append((way, n - 1))
 
-        def moe(which, offset):
+        def layer_rows(which, offset):
             base = pl.ds(pl.multiple_of(p.z * chip_rows + offset * my_rows, my_rows), my_rows)
             value = part[j, base]
             for way, slot in ends:
                 value = value + red_recv[j, way, slot, which].astype(jnp.float32)
-            return value.astype(jnp.bfloat16)
-
-        moe_send[j] = moe(their_rows, 1 - c)
+            moe = value.astype(jnp.bfloat16).astype(jnp.float32)
+            before = after_mix[which, j * fc : (j + 1) * fc].astype(jnp.float32)
+            return (before + moe).astype(jnp.bfloat16)
+
+        moe_send[j] = layer_rows(their_rows, 1 - c)
         give_rows(j).start()
-        value = after_mix[:, cols(c, j)].astype(jnp.float32) + moe(own_rows, c).astype(jnp.float32)
-        out[:, cols(c, j)] = value.astype(jnp.bfloat16)
+        out[:, cols(c, j)] = layer_rows(own_rows, c)
 
     def take_rows(j):
         give_rows(j).wait_recv()
-        value = after_mix[:, cols(1 - c, j)].astype(jnp.float32) + moe_recv[j].astype(jnp.float32)
-        out[:, cols(1 - c, j)] = value.astype(jnp.bfloat16)
+        out[:, cols(1 - c, j)] = moe_recv[j]
 
     down(0)
     for j in range(1, nc):
@@ -469,11 +681,63 @@
     return pl.BlockSpec(memory_space=pl.ANY)
 
 
+def mix(queries, keys, values, sink, w_out, residual, gain, ids, weights, capacity):
+    nc = CHUNKS
+    rows = queries.shape[0]
+    my_rows, width = residual.shape
+    half = width // 2
+    fc = half // nc
+    tp_count, sp_count = lax.axis_size("tp"), lax.axis_size("sp")
+    experts = sp_count * tp_count // 2
+    slots = sp_count * capacity
+    hops = tp_count // 4
+    bf, f32 = jnp.bfloat16, jnp.float32
+    dma = pltpu.SemaphoreType.DMA
+    return pl.pallas_call(
+        mix_kernel,
+        name="mix",
+        out_shape=(
+            jax.ShapeDtypeStruct((2 * my_rows, half), bf),
+            jax.ShapeDtypeStruct((2 * my_rows, half), bf),
+            jax.ShapeDtypeStruct((slots, rows), bf),
+            jax.ShapeDtypeStruct((rows, slots), bf),
+        ),
+        in_specs=[vmem()] * 9,
+        out_specs=(vmem(),) * 4,
+        scratch_shapes=[
+            pltpu.VMEM((rows + WINDOW, 128), bf),
+            pltpu.VMEM((rows + WINDOW, 128), bf),
+            pltpu.VMEM((rows // WINDOW, HD, WINDOW), bf),
+            pltpu.VMEM((tp_count * HD, 2 * my_rows), bf),
+            pltpu.VMEM((2 * my_rows, tp_count * HD), bf),
+            pltpu.VMEM((nc, tp_count * HD, fc), bf),
+            pltpu.VMEM((2 * my_rows, half), bf),
+            pltpu.VMEM((2 * my_rows, 128), f32),
+            pltpu.VMEM((2 * my_rows, 128), f32),
+            pltpu.VMEM((rows, experts), bf),
+            pltpu.VMEM((rows, experts), bf),
+            dma((2,)),
+            dma((2,)),
+            dma((1,)),
+            dma((1,)),
+            dma((nc,)),
+            dma((nc,)),
+            dma((nc, 2, hops)),
+            dma((nc, 2, hops)),
+            dma((1,)),
+            dma((1,)),
+            dma((1,)),
+            dma((1,)),
+        ],
+        compiler_params=pltpu.CompilerParams(collective_id=3, has_side_effects=True),
+    )(queries, keys, values, sink, w_out, residual, gain, ids, weights)
+
+
 def dispatch(normed, pick, w_gate, w_up, shared_gate, shared_up):
     nc = CHUNKS
     slots, rows = pick.shape
-    width = normed.shape[1]
-    half = width // 2
+    half = normed.shape[1]
+    width = 2 * half
     fc = half // nc
     hidden_units, units = w_gate.shape[0], shared_gate.shape[0]
     hops = lax.axis_size("tp") // 4
@@ -501,8 +765,6 @@
             pltpu.VMEM((rows, 4 * units), f32),
             pltpu.VMEM((rows, 4 * units), f32),
             dma((2,)),
-            dma((nc,)),
-            dma((nc,)),
             dma((nc, 2, hops)),
             dma((nc, 2, hops)),
             dma((nc,)),
@@ -519,8 +781,8 @@
 def combine(hidden, w_down, blend, shared, shared_down, after_mix):
     nc = CHUNKS
     rows, slots = blend.shape
-    my_rows, width = after_mix.shape
-    half = width // 2
+    my_rows, half = after_mix.shape[0] // 2, after_mix.shape[1]
+    width = 2 * half
     fc = half // nc
     hidden_units, units = w_down.shape[0], shared_down.shape[0]
     hops = lax.axis_size("tp") // 4
@@ -560,27 +822,6 @@
     )(hidden, w_down, blend, shared, shared_down, after_mix)
 
 
-def slot_matrices(ids, weights, experts, capacity, lanes, lane):
-    rows = ids.shape[0]
-    slots = experts // lanes * capacity
-    named = ids[:, :, None] == jnp.arange(experts, dtype=jnp.int32)
-    weight = jnp.sum(jnp.where(named, weights[:, :, None], 0.0), axis=1)
-    named = jnp.any(named, axis=1)
-    index = jnp.arange(rows, dtype=jnp.int32)
-    before = (index[None, :] < index[:, None]).astype(jnp.bfloat16)
-    rank = dot_nn(before, named.astype(jnp.bfloat16))
-    rank = jnp.where(named, rank, -1.0).astype(jnp.bfloat16)
-    slot = jnp.arange(slots, dtype=jnp.int32)
-    holds = slot[:, None] // capacity * lanes + lane == jnp.arange(experts, dtype=jnp.int32)
-    holds = holds.astype(jnp.bfloat16)
-    place = (slot % capacity).astype(jnp.float32)
-    pick = (dot_nt(holds, rank) == place[:, None]).astype(jnp.bfloat16)
-    blend = jnp.where(
-        dot_nt(rank, holds) == place[None, :], dot_nt(weight.astype(jnp.bfloat16), holds), 0.0
-    )
-    return pick, blend.astype(jnp.bfloat16)
-
-
 def body(
     queries,
     keys,
@@ -598,60 +839,17 @@
     shared_up,
     shared_down,
 ):
-    tp_count = lax.axis_size("tp")
-    sp_count = lax.axis_size("sp")
-    seq_rows = queries.shape[0]
-    expert_count = sp_count * tp_count // 2
-    capacity = CAP
-    local_heads = queries.shape[1] // HD
-    kv_start = lax.axis_index("tp") * local_heads // GROUP * HD
-    key_cols = lax.dynamic_slice_in_dim(keys, kv_start, HD, 1)
-    value_cols = lax.dynamic_slice_in_dim(values, kv_start, HD, 1)
-    rim_keys, rim_values = shifted(
-        (key_cols[seq_rows - WINDOW :], value_cols[seq_rows - WINDOW :]), "sp", 1
-    )
-    num_blocks = seq_rows // WINDOW
-    key_blocks = key_cols.reshape(num_blocks, WINDOW, HD)
-    value_blocks = value_cols.reshape(num_blocks, WINDOW, HD)
-    keys_ext = jnp.concatenate(
-        [jnp.concatenate([rim_keys[None], key_blocks[:-1]], axis=0), key_blocks], axis=1
-    )
-    values_ext = jnp.concatenate(
-        [jnp.concatenate([rim_values[None], value_blocks[:-1]], axis=0), value_blocks], axis=1
-    )
-    query_blocks = queries.reshape(num_blocks, WINDOW, local_heads, HD)
-    scores = jnp.einsum(
-        "nqhd,nsd->nhqs", query_blocks, keys_ext, preferred_element_type=jnp.float32
-    ) * HD ** (-0.5)
-    query_pos = jnp.arange(WINDOW)[:, None] + WINDOW
-    key_pos = jnp.arange(2 * WINDOW)[None, :]
-    in_band = (key_pos <= query_pos) & (key_pos > query_pos - WINDOW)
-    absolute = (
-        lax.axis_index("sp") * seq_rows
-        + jnp.arange(num_blocks)[:, None, None] * WINDOW
-        + key_pos[None]
-        - WINDOW
-    )
-    allowed = in_band[None] & (absolute >= 0)
-    scores = jnp.where(allowed[:, None], scores, -jnp.inf)
-    sink_col = jnp.broadcast_to(sink_logits[None, :, None, None], scores.shape[:-1] + (1,))
-    combined = jnp.concatenate([scores, sink_col], axis=-1)
-    row_max = jnp.max(combined, axis=-1, keepdims=True)
-    exps = jnp.exp(combined - row_max)
-    weights = (exps[..., :-1] / jnp.sum(exps, axis=-1, keepdims=True)).astype(jnp.bfloat16)
-    attended = jnp.einsum("nhqs,nsd->nqhd", weights, values_ext, preferred_element_type=jnp.float32)
-    attended = attended.astype(jnp.bfloat16).reshape(seq_rows, local_heads * HD)
-    head_rows = lax.all_to_all(attended, "tp", split_axis=0, concat_axis=1, tiled=True)
-    projected = jnp.dot(
-        head_rows,
-        lax.all_gather(w_out, "tp", axis=0, tiled=True),
-        preferred_element_type=jnp.float32,
-    )
-    after_mix = (residual.astype(jnp.float32) + projected).astype(jnp.bfloat16)
-    normed = normalize(after_mix, norm_gain)
-    lanes = tp_count // 2
-    pick, blend = slot_matrices(
-        expert_ids, expert_weights, expert_count, capacity, lanes, lax.axis_index("tp") // 2
+    normed, after_mix, pick, blend = mix(
+        queries,
+        keys,
+        values,
+        sink_logits[:, None],
+        w_out,
+        residual,
+        norm_gain[None, :],
+        expert_ids,
+        expert_weights,
+        CAP,
     )
     hidden, shared = dispatch(normed, pick, w_gate[0], w_up[0], shared_gate, shared_up)
     return combine(hidden, w_down[0], blend, shared, shared_down, after_mix)

time: 186 us -> 169 us (0.909); the launches traced: 186 us -> 166 us
  Pallas kernels: 116 us -> 159 us
  waiting for transfers between devices: 20.8 us -> 0 us
  starting transfers between devices: 16.8 us -> 0 us
  between operations: 14.4 us -> 0.68 us
  matrix products: 9.73 us -> 0 us
  other arithmetic: 3.55 us -> 0 us
  local copies, waits for them, and re-layouts: 4.7 us -> 6.9 us
    pallas_call x0 -> x1, Pallas kernels: none -> 45.7 us  [mix(): pl.pallas_call(mix_kernel, name='mix', out_shape=(jax.ShapeDtypeStruct((2...]
    all_gather x1 -> x0, waiting for transfers between devices: 11.7 us -> none  [body(): lax.all_gather(w_out, 'tp', axis=0, tiled=True)]
    dot_general x7 -> x0, matrix products: 9.73 us -> none  [the longest x3 5.06 us: dot_nt(): lax.dot_general(a, b, (((1,), (1,)), ((), ())), preferred_element_type=jn...]
    all_to_all x1 -> x0, starting transfers between devices: 9.71 us -> none  [body(): lax.all_to_all(attended, 'tp', split_axis=0, concat_axis=1, tiled=True)]
    all_to_all x1 -> x0, waiting for transfers between devices: 8.4 us -> none  [body(): lax.all_to_all(attended, 'tp', split_axis=0, concat_axis=1, tiled=True)]
    ppermute x2 -> x0, starting transfers between devices: 7.05 us -> none  [shifted(): return lax.ppermute(block, axis, route)]
    unnamed x17 -> x4, local copies, waits for them, and re-layouts: 3.06 us -> 6.9 us
    pallas_call x1, Pallas kernels: 63 us -> 60.3 us  [dispatch(): pl.pallas_call(dispatch_kernel, name='dispatch', out_shape=(jax.ShapeDtyp...]
  transfers between devices with their start and end apart: 4 -> 0, of which waited for: 2 -> 0; matrix products, arithmetic and copies ran while one was open for 7% -> 0% of each run, Pallas kernels for 0% -> 0%
where the time goes in v2:
time: 169 us; the launch traced here: 166 us
  Pallas kernels  159 us (94%)
  local copies, waits for them, and re-layouts  6.9 us (4%)
    pallas_call x1, Pallas kernels, dispatch(): pl.pallas_call(dispatch_kernel, name='dispatch', out_shape=(jax.ShapeDtyp...  60.3 us
    pallas_call x1, Pallas kernels, combine(): pl.pallas_call(combine_kernel, name='combine', out_shape=jax.ShapeDtypeSt...  52.9 us
    pallas_call x1, Pallas kernels, mix(): pl.pallas_call(mix_kernel, name='mix', out_shape=(jax.ShapeDtypeStruct((2...  45.7 us
    unnamed x4, local copies, waits for them, and re-layouts  6.9 us

profile of v2, /device:TPU:1, one launch (start us, length us, event | category | flops | bytes accessed | tf_op | source)
XLA Modules:
  0.0 166.5 jit_solution(9856665155356658898)
XLA Ops:
  0.7 1.7 %copy.16.queries = bf16[1024,64]{1,0:T(8,128)(2,1)} copy(bf16[1024,64]{0,1:T(8,128)(2,1)} %param.15) | data formatting | bytes 262144 | tf_op args[0]
  2.4 1.7 %copy.17.ids = s32[1024,4]{1,0:T(8,128)} copy(s32[1024,4]{0,1:T(4,128)} %param.22) | data formatting | bytes 32768 | tf_op args[7]
  4.1 1.8 %copy.18.weights = f32[1024,4]{1,0:T(8,128)} copy(f32[1024,4]{0,1:T(4,128)} %param.23) | data formatting | bytes 32768 | tf_op args[8]
  5.9 45.7 %mix.1 = (bf16[128,1024]{1,0:T(8,128)(2,1)}, bf16[128,1024]{1,0:T(8,128)(2,1)}, bf16[1024,1024]{1,0:T(8,128)(2,1)}, bf16[1024,1024]{1,0:T(8,128)(2,1)}) custom-call(bf16[1024,64]{1,0:T(8,128)(2,1)} %copy.16.queries, bf16[1024,256]{1,0:T(8,128)(2,1)} %keys.1, bf16[1024,256]{1,0:T(8,128)(2,1)} %values.1, f32[1,1]{1,0:T(1,128)} %bitcast.5.sink, ...), custom_call_target="tpu_custom_call" | custom-call | tf_op jit(solution)/shard_map/mix/pallas_call | solution.py:696
  51.6 60.3 %dispatch.1 = (bf16[1024,768]{1,0:T(8,128)(2,1)}, bf16[1024,64]{1,0:T(8,128)(2,1)}) custom-call(bf16[128,1024]{1,0:T(8,128)(2,1)} %get-tuple-element.11.normed, bf16[1024,1024]{1,0:T(8,128)(2,1)} %get-tuple-element.12.pick, bf16[768,2048]{1,0:T(8,128)(2,1)} %bitcast.6, bf16[768,2048]{1,0:T(8,128)(2,1)} %bitcast.7, bf16[32,2048]{1,0:T(8,128)(2,1)} %sg.1, ...), custom_call_target="tpu_custom_call" | custom-call | tf_op jit(solution)/shard_map/dispatch/pallas_call | solution.py:746
  111.9 52.9 %combine.1 = bf16[64,2048]{1,0:T(8,128)(2,1)} custom-call(bf16[1024,768]{1,0:T(8,128)(2,1)} %get-tuple-element.13.hidden, bf16[768,2048]{1,0:T(8,128)(2,1)} %bitcast.8, bf16[1024,1024]{1,0:T(8,128)(2,1)} %get-tuple-element.14.blend, bf16[1024,64]{1,0:T(8,128)(2,1)} %get-tuple-element.15.shared, bf16[32,2048]{1,0:T(8,128)(2,1)} %sd.1, ...), custom_call_target="tpu_custom_call" | custom-call | tf_op jit(solution)/shard_map/combine/pallas_call | solution.py:791
  164.8 1.7 %copy.21 = bf16[64,2048]{1,0:T(8,128)(2,1)} copy(bf16[64,2048]{1,0:T(8,128)(2,1)} %combine.1) | data formatting | bytes 524288

commit v3 on v0

v3 whole, which is shorter than its diff:
```python
import jax
import jax.numpy as jnp
from jax import lax
from jax.experimental import pallas as pl
from jax.experimental.pallas import tpu as pltpu
from jax.sharding import PartitionSpec as P

HD = 64
GROUP = 4
WINDOW = 128
TOPK = 4


MESH = pl.DeviceIdType.MESH
CHUNKS = 4
CUTS = (2, 2, 2, 1, 1)
CAP = 64


def dot_nt(a, b):
    return lax.dot_general(a, b, (((1,), (1,)), ((), ())), preferred_element_type=jnp.float32)


def dot_nn(a, b):
    return jnp.dot(a, b, preferred_element_type=jnp.float32)


def rows_loop(total, step, fn):
    def one(i, carry):
        fn(pl.ds(pl.multiple_of(i * step, step), step))
        return carry

    lax.fori_loop(0, total // step, one, 0)


class Place:
    def __init__(self):
        self.sp_count = lax.axis_size("sp")
        self.tp_count = lax.axis_size("tp")
        self.s = lax.axis_index("sp")
        self.t = lax.axis_index("tp")
        self.c = self.t % 2
        self.z = self.t // 2
        self.nz = self.tp_count // 2
        self.partner = (self.s, self.t + 1 - 2 * self.c)
        self.right = (self.s, (self.t + 2) % self.tp_count)
        self.left = (self.s, (self.t + self.tp_count - 2) % self.tp_count)

    def peer(self, o):
        return ((self.s + o) % self.sp_count, self.t)

    def barrier(self):
        sem = pltpu.get_barrier_semaphore()

        def greet(count, device):
            def one(o, carry):
                pl.semaphore_signal(sem, inc=1, device_id=device(o), device_id_type=MESH)
                return carry

            lax.fori_loop(1, count, one, 0)

        greet(self.tp_count, lambda o: (self.s, (self.t + o) % self.tp_count))
        greet(self.sp_count, self.peer)
        pl.semaphore_wait(sem, self.tp_count + self.sp_count - 2)

    def steps(self, j):
        far, near = self.nz // 2, self.nz - 1 - self.nz // 2
        return (far, near) if j % 2 == 0 else (near, far)


def remote(src, dst, send_sem, recv_sem, device):
    return pltpu.make_async_remote_copy(
        src_ref=src, dst_ref=dst, send_sem=send_sem, recv_sem=recv_sem, device_id=device, device_id_type=MESH
    )


class RingGather:
    def __init__(self, p, buf, rows, send_sems, recv_sems):
        self.p, self.buf, self.rows = p, buf, rows
        self.ss, self.rs = send_sems, recv_sems

    def copy(self, j, way, k, shift):
        p = self.p
        origin = (p.z - shift if way == 0 else p.z + shift) + p.nz
        block = self.buf.at[j, pl.ds(pl.multiple_of(origin % p.nz * self.rows, self.rows), self.rows)]
        return remote(block, block, self.ss.at[j, way, k - 1], self.rs.at[j, way, k - 1], p.left if way else p.right)

    def send(self, j, k):
        for way in range(2):
            if k <= self.p.steps(j)[way]:
                self.copy(j, way, k, k - 1).start()

    def wait(self, j, k):
        for way in range(2):
            if k <= self.p.steps(j)[way]:
                self.copy(j, way, k, k).wait_recv()

    def drain(self, j):
        for way in range(2):
            for k in range(1, self.p.steps(j)[way] + 1):
                self.copy(j, way, k, k - 1).wait_send()


class Exchange:
    def __init__(self, p, src, dst, rows, spans, send_sems, recv_sems):
        self.p, self.src, self.dst, self.rows, self.spans = p, src, dst, rows, spans
        self.ss, self.rs = send_sems, recv_sems

    def block(self, index, j):
        return pl.ds(pl.multiple_of(index * self.rows, self.rows), self.rows), self.spans[j]

    def send(self, j):
        p = self.p

        def one(o, carry):
            peer = p.peer(o)
            remote(
                self.src.at[self.block(peer[0], j)],
                self.dst.at[self.block(p.s, j)],
                self.ss.at[j],
                self.rs.at[j],
                peer,
            ).start()
            return carry

        lax.fori_loop(1, p.sp_count, one, 0)
        self.dst[self.block(p.s, j)] = self.src[self.block(p.s, j)]

    def all_of(self, j):
        others = pl.ds(0, (self.p.sp_count - 1) * self.rows), self.spans[j]
        return remote(self.src.at[others], self.dst.at[others], self.ss.at[j], self.rs.at[j], self.p.peer(1))

    def wait(self, j):
        self.all_of(j).wait_recv()

    def drain(self, j):
        self.all_of(j).wait_send()


def iota(shape, axis):
    return lax.broadcasted_iota(jnp.int32, shape, axis)


def silu_times(gate, up):
    return (gate / (1.0 + jnp.exp(-gate)) * up).astype(jnp.bfloat16)


def layer_kernel(
    queries, keys, values, sink, w_out, residual, gain, ids, weights, wg_hbm, wu_hbm, wd_hbm, sg, su, sd,
    out,
    key_ext, value_ext, att, heads, heads_t, wide, res, after, square, square_other,
    rank_buf, rank_t, weight_buf, pick, blend, scale_rows, scale_cols, scale_slots,
    ring_buf, outgoing, own, other, wg, wu, gate_sum, up_sum, sgu, pre, pre_other, hidden, shared,
    wd, half_send, half_recv, total, held, sdh, part, red_send, red_recv, far_send, far_recv, row_send, row_recv,
    w_sem, k_send, k_recv, h_send, h_recv, x_send, x_recv, o_send, o_recv, r_send, r_recv, q_send, q_recv,
    g_send, g_recv, a_send, a_recv, f_send, f_recv, s_send, s_recv,
    d_send, d_recv, t_send, t_recv, b_send, b_recv, e_send, e_recv, m_send, m_recv, n_send, n_recv, z_send, z_recv,
):
    p = Place()
    c, nc = p.c, CHUNKS
    rows = queries.shape[1]
    my_rows, width = residual.shape
    half = width // 2
    fc = half // nc
    head_rows = w_out.shape[0]
    chip_rows = 2 * my_rows
    blocks = rows // WINDOW
    experts = p.sp_count * p.nz
    slots = pick.shape[0]
    capacity = slots // p.sp_count
    units = sg.shape[0]
    tile = min(256, rows, slots)
    last = p.nz // 2
    everything = tuple(range(nc))
    kv = p.t // GROUP
    kv_cols = pl.ds(pl.multiple_of(kv // 2 * 128, 128), 128)
    f32, bf = jnp.float32, jnp.bfloat16

    def half_of(h):
        return pl.ds(pl.multiple_of(h * half, half), half)

    def cols(h, j):
        return pl.ds(pl.multiple_of(h * half + j * fc, fc), fc)

    pairs = ((wg_hbm, wg), (wu_hbm, wu), (wd_hbm, wd))
    fetches = [pltpu.make_async_copy(src, dst, w_sem.at[i]) for i, (src, dst) in enumerate(pairs)]
    for copy in fetches:
        copy.start()
    p.barrier()

    def shard(core):
        return pl.ds(pl.multiple_of(p.z * 2 * head_rows + core * head_rows, head_rows), head_rows)

    def swap(j, core):
        return remote(
            w_out.at[:, cols(1 - c, j)], wide.at[j, shard(core)], x_send.at[j], x_recv.at[j], p.partner
        )

    rim = pl.ds(rows - WINDOW, WINDOW)
    following = ((p.s + 1) % p.sp_count, p.t)
    halo = [
        remote(ref.at[rim, kv_cols], ext.at[pl.ds(0, WINDOW)], k_send.at[i], k_recv.at[i], following)
        for i, (ref, ext) in enumerate(((keys, key_ext), (values, value_ext)))
    ]
    sends_rim, gets_rim = p.s + 1 < p.sp_count, p.s > 0

    def part_of(core):
        return pl.ds(pl.multiple_of(core * my_rows, my_rows), my_rows)

    def swap_res(core):
        return remote(residual.at[:, half_of(1 - c)], res.at[part_of(core)], r_send.at[0], r_recv.at[0], p.partner)

    unit_rows = [pl.ds(pl.multiple_of(k * 2 * units + c * units, units), units) for k in range(2)]
    my_units = pl.ds(pl.multiple_of(c * units, units), units)
    shared_swaps = [
        remote(sg.at[:, half_of(1 - c)], sgu.at[unit_rows[0]], s_send.at[0], s_recv.at[0], p.partner),
        remote(su.at[:, half_of(1 - c)], sgu.at[unit_rows[1]], s_send.at[1], s_recv.at[1], p.partner),
        remote(sd.at[:, half_of(1 - c)], sdh.at[my_units], d_send.at[0], d_recv.at[0], p.partner),
    ]
    for j in everything:
        swap(j, c).start()

    @pl.when(sends_rim)
    def _():
        for copy in halo:
            copy.start()

    swap_res(c).start()
    for copy in shared_swaps:
        copy.start()
    for j in everything:
        wide[j, shard(c)] = w_out[:, cols(c, j)]
    ring = RingGather(p, wide, 2 * head_rows, o_send, o_recv)
    for j in everything:
        swap(j, 1 - c).wait_recv()
        ring.send(j, 1)
    hops = iter([(j, k) for k in range(1, last) for j in everything])

    def hop(count=1):
        for _ in range(count):
            event = next(hops, None)
            if event is not None:
                ring.wait(*event)
                ring.send(event[0], event[1] + 1)

    key_ext[pl.ds(WINDOW, rows)] = keys[:, kv_cols]
    value_ext[pl.ds(WINDOW, rows)] = values[:, kv_cols]
    res[part_of(c)] = residual[:, half_of(c)]
    sgu[unit_rows[0]] = sg[:, half_of(c)]
    sgu[unit_rows[1]] = su[:, half_of(c)]
    sdh[my_units] = sd[:, half_of(c)]

    @pl.when(gets_rim)
    def _():
        for copy in halo:
            copy.wait_recv()

    @pl.when(jnp.logical_not(gets_rim))
    def _():
        key_ext[pl.ds(0, WINDOW)] = jnp.zeros((WINDOW, 128), bf)
        value_ext[pl.ds(0, WINDOW)] = jnp.zeros((WINDOW, 128), bf)

    lane_half = kv % 2
    sink_value = sink[...]
    head_place = pl.ds(pl.multiple_of(p.t * HD, HD), HD)

    def head_piece(b, device):
        return remote(att.at[b], heads.at[head_place], h_send.at[0], h_recv.at[0], device)

    others = heads.at[pl.ds(0, (p.tp_count - 1) * HD)]
    head_total = remote(others, others, h_send.at[0], h_recv.at[0], p.partner)

    def attend(i):
        b = (p.z + i) % blocks
        here = pl.ds(pl.multiple_of(b * WINDOW, WINDOW), WINDOW)
        ext = pl.ds(pl.multiple_of(b * WINDOW, WINDOW), 2 * WINDOW)
        query = queries[:, here].astype(f32)
        query = jnp.concatenate([query, query], axis=0)
        in_half = jnp.right_shift(iota((2 * HD, WINDOW), 0), HD.bit_length() - 1) == lane_half
        query = jnp.where(in_half, query, 0.0).astype(bf)
        scores = dot_nn(key_ext[ext], query) * HD ** (-0.5)
        key_pos = iota((2 * WINDOW, WINDOW), 0)
        query_pos = iota((2 * WINDOW, WINDOW), 1) + WINDOW
        first_key = jnp.where(p.s * blocks + b == 0, WINDOW, 0)
        allowed = (key_pos <= query_pos) & (key_pos > query_pos - WINDOW) & (key_pos >= first_key)
        scores = jnp.where(allowed, scores, -jnp.inf)
        top = jnp.maximum(jnp.max(scores, axis=0, keepdims=True), sink_value)
        exps = jnp.exp(scores - top)
        full = jnp.sum(exps, axis=0, keepdims=True) + jnp.exp(sink_value - top)
        shares = (exps / full).astype(bf)
        both = lax.dot_general(
            value_ext[ext], shares, (((0,), (0,)), ((), ())), preferred_element_type=f32
        )
        att[b] = jnp.where(lane_half == 0, both[:HD], both[HD:]).astype(bf)
        for core in range(2):
            target = 2 * b + core

            @pl.when(target != p.t)
            def _():
                head_piece(b, (p.s, target)).start()

            @pl.when(target == p.t)
            def _():
                heads[head_place] = att[b]

    def attend_some(first, count):
        def one(i, carry):
            attend(i)
            return carry

        lax.fori_loop(first, first + count, one, 0)

    quarter = max(1, blocks // 4)
    for i in range(0, blocks, quarter):
        attend_some(i, quarter)
        hop(1 if i == 0 else 2)

    shift = capacity.bit_length() - 1

    def name_rows(i, carry):
        span = pl.ds(pl.multiple_of(i * tile, tile), tile)
        expert = iota((experts, tile), 0)
        named = jnp.zeros((experts, tile), f32)
        weight = jnp.zeros((experts, tile), f32)
        tile_ids, tile_weights = ids[:, span], weights[:, span]
        for k in range(TOPK):
            same = tile_ids[k : k + 1] == expert
            named = jnp.where(same, 1.0, named)
            weight = jnp.where(same, tile_weights[k : k + 1], weight)
        rank_t[:, span] = named.astype(bf)
        weight_buf[span] = weight.T.astype(bf)
        return carry

    lax.fori_loop(0, rows // tile, name_rows, 0)
    hop()
    all_named = rank_t[...]
    ranks = []
    for i in range(rows // tile):
        before = iota((rows, tile), 0) < iota((rows, tile), 1) + i * tile
        rank = dot_nn(all_named, jnp.where(before, 1.0, 0.0).astype(bf))
        named = all_named[:, i * tile : (i + 1) * tile].astype(f32) > 0.0
        ranks.append(jnp.where(named, rank, -1.0))
    for i, rank in enumerate(ranks):
        rank_t[:, i * tile : (i + 1) * tile] = rank.astype(bf)
        rank_buf[i * tile : (i + 1) * tile] = rank.T.astype(bf)
    hop()

    def holds(first, count):
        slot = iota((count, experts), 0) + first
        same = jnp.right_shift(slot, shift) * p.nz + p.z == iota((count, experts), 1)
        return jnp.where(same, 1.0, 0.0).astype(bf)

    def fill_pick(r, first):
        place = jnp.bitwise_and(iota((tile, rows), 0) + first, capacity - 1).astype(f32)
        hit = dot_nn(holds(first, tile), rank_t[...]) == place
        pick[r] = jnp.where(hit, 1.0, 0.0).astype(bf)

    for i in range(slots // tile):
        fill_pick(pl.ds(i * tile, tile), i * tile)
        hop()

    def fill_blend(r):
        all_holds = holds(0, slots)
        place = jnp.bitwise_and(iota((tile, slots), 1), capacity - 1).astype(f32)
        hit = dot_nt(rank_buf[r], all_holds) == place
        blend[r] = jnp.where(hit, dot_nt(weight_buf[r], all_holds), 0.0).astype(bf)

    def fill_blend_tiles(first, end):
        for i in range(first, end):
            fill_blend(pl.ds(i * tile, tile))

    hop(nc * last)

    head_total.wait_recv()
    heads_t[...] = heads[...].T
    swap_res(1 - c).wait_recv()
    chip_place = pl.ds(pl.multiple_of(p.z * chip_rows, chip_rows), chip_rows)
    gather = RingGather(p, ring_buf, chip_rows, g_send, g_recv)
    squares = jnp.zeros((chip_rows, 1), f32)
    for j in everything:
        ring.wait(j, last)
        piece = pl.ds(j * fc, fc)
        mixed = (res[:, piece].astype(f32) + dot_nn(heads_t[...], wide[j])).astype(bf)
        after[:, piece] = mixed
        ring_buf[j, chip_place] = mixed
        gather.send(j, 1)
        mixed = mixed.astype(f32)
        squares = squares + jnp.sum(mixed * mixed, axis=1, keepdims=True)
    square[...] = jnp.broadcast_to(squares, square.shape)
    swap_square = remote(square, square_other, q_send.at[0], q_recv.at[0], p.partner)
    swap_square.start()
    fill_blend_tiles(0, 1)
    swap_square.wait_recv()
    mean = (square[...] + square_other[...]) / width
    scale_rows[p.z] = lax.rsqrt(mean + 1e-06).T[:8]

    def send_scale(o):
        mine = scale_rows.at[p.z]
        return remote(mine, mine, n_send.at[0], n_recv.at[0], (p.s, (p.t + 2 * o) % p.tp_count))

    for o in range(1, p.nz):
        send_scale(o).start()
    all_scales = scale_rows.at[pl.ds(0, p.nz - 1)]
    scale_total = remote(all_scales, all_scales, n_send.at[0], n_recv.at[0], p.partner)

    def take_scales():
        scale_total.wait_recv()
        for z in range(p.nz):
            block = jnp.broadcast_to(scale_rows[z, :1], (128, chip_rows))
            scale_cols[z * chip_rows : (z + 1) * chip_rows] = block.T
        flat = jnp.concatenate([scale_rows[z, :1] for z in range(p.nz)], axis=1)

        def one(r):
            found = jnp.sum(pick[r].astype(f32) * flat, axis=1, keepdims=True)
            scale_slots[r] = jnp.broadcast_to(found, (tile, 128))

        rows_loop(slots, tile, one)

    even = [pl.ds(j * fc, fc) for j in everything]
    spread = Exchange(p, outgoing, own, capacity, even, a_send, a_recv)

    def forward(j):
        return remote(own.at[:, even[j]], other.at[:, even[j]], f_send.at[j], f_recv.at[j], p.partner)

    def pass_on(pair, k):
        for j in pair:
            gather.wait(j, k)
            gather.send(j, k + 1)

    def select(j):
        gather.wait(j, last)

        def one(r):
            value = dot_nn(pick[r], ring_buf[j]) * scale_slots[r][:, :1] * gain[:, cols(c, j)]
            outgoing[r, even[j]] = value.astype(bf)

        rows_loop(slots, tile, one)
        spread.send(j)

    def shared_part(j):
        def one(r):
            normed = ring_buf[j, r].astype(f32) * scale_cols[r][:, :1] * gain[:, cols(c, j)]
            value = dot_nt(normed.astype(bf), sgu[:, j * fc : (j + 1) * fc])
            pre[r] = value if j == 0 else pre[r] + value

        rows_loop(rows, tile, one)

    def arrive(j):
        spread.wait(j)
        forward(j).start()

    def multiply(j):
        forward(j).wait_recv()

        def one(r):
            a, b = own[r, even[j]], other[r, even[j]]
            for w, acc in ((wg, gate_sum), (wu, up_sum)):
                value = dot_nt(a, w[:, cols(c, j)]) + dot_nt(b, w[:, cols(1 - c, j)])
                acc[r] = value if j == 0 else acc[r] + value

        rows_loop(slots, tile, one)

    for k in range(1, last):
        pass_on(everything, k)
        if k == 1:
            fill_blend_tiles(1, rows // tile)
            take_scales()
    if last == 1:
        fill_blend_tiles(1, rows // tile)
        take_scales()
    for copy in shared_swaps:
        copy.wait_recv()
    for j in everything:
        select(j)
    for j in (0, 1):
        shared_part(j)
    arrive(0)
    for copy in fetches[:2]:
        copy.wait()
    multiply(0)
    for j in (2, 3):
        shared_part(j)
    swap_pre = remote(pre, pre_other, s_send.at[2], s_recv.at[2], p.partner)
    swap_pre.start()
    arrive(1)
    swap_pre.wait_recv()

    def shared_one(r):
        both = pre[r] + pre_other[r]
        shared[r] = silu_times(both[:, : 2 * units], both[:, 2 * units :])

    rows_loop(rows, tile, shared_one)
    multiply(1)
    arrive(2)
    multiply(2)
    arrive(3)
    multiply(3)

    def hidden_one(r):
        hidden[r] = silu_times(gate_sum[r], up_sum[r])

    rows_loop(slots, tile, hidden_one)

    fetches[2].wait()
    unit = half // sum(CUTS)
    starts = [sum(CUTS[:j]) * unit for j in range(len(CUTS))]
    sizes = [cut * unit for cut in CUTS]
    spans = [pl.ds(a, n) for a, n in zip(starts, sizes)]
    count = len(CUTS)
    back = Exchange(p, total, held, capacity, spans, b_send, b_recv)

    def span_of(h, j):
        return pl.ds(pl.multiple_of(h * half + starts[j], unit), sizes[j])

    def give(j):
        return remote(half_send.at[:, spans[j]], half_recv.at[:, spans[j]], t_send.at[j], t_recv.at[j], p.partner)

    def down(j):
        def theirs(r):
            half_send[r, spans[j]] = dot_nn(hidden[r], wd[:, span_of(1 - c, j)]).astype(bf)

        def ours(r):
            total[r, spans[j]] = dot_nn(hidden[r], wd[:, span_of(c, j)]).astype(bf)

        rows_loop(slots, tile, theirs)
        give(j).start()
        rows_loop(slots, tile, ours)

    def add_halves(j):
        give(j).wait_recv()

        def one(r):
            both = total[r, spans[j]].astype(f32) + half_recv[r, spans[j]].astype(f32)
            total[r, spans[j]] = both.astype(bf)

        rows_loop(slots, tile, one)
        back.send(j)

    def blend_rows(j):
        back.wait(j)

        def one(r):
            mixed = dot_nn(blend[r], held[:, spans[j]])
            part[r, spans[j]] = mixed + dot_nn(shared[r], sdh[:, spans[j]])

        rows_loop(rows, tile, one)

    def chip_block(distance):
        index = (p.z + distance + p.nz) % p.nz
        return pl.ds(pl.multiple_of(index * chip_rows, chip_rows), chip_rows)

    def red(j, way, m):
        sems = e_send.at[j, way, m - 1], e_recv.at[j, way, m - 1]
        refs = [ref.at[way, m - 1, :, spans[j]] for ref in (red_send, red_recv)]
        return remote(*refs, *sems, p.left if way else p.right)

    def step(j, m):
        for way in range(2):
            n = p.steps(j)[way]
            if m > n:
                continue
            distance = n - m + 1
            value = part[chip_block(-distance if way else distance), spans[j]]
            if m > 1:
                red(j, way, m - 1).wait_recv()
                value = value + red_recv[way, m - 2, :, spans[j]].astype(f32)
            red_send[way, m - 1, :, spans[j]] = value.astype(bf)
            red(j, way, m).start()

    def far(o):
        device = (p.s, (p.t + 2 * o) % p.tp_count)
        return remote(far_send.at[o - 1], far_recv.at[o - 1], z_send.at[o - 1], z_recv.at[o - 1], device)

    def send_far(j):
        for o in (o for o in sorted(range(1, p.nz), key=lambda o: -min(o, p.nz - o))):
            far_send[o - 1] = part[chip_block(o), spans[j]].astype(bf)
            far(o).start()

    def give_rows(j):
        return remote(row_send.at[:, spans[j]], row_recv.at[:, spans[j]], m_send.at[j], m_recv.at[j], p.partner)

    def finish(j):
        ends = []
        if j == count - 1:
            for o in range(1, p.nz):
                far(o).wait_recv()
                ends.append(far_recv.at[o - 1])
        else:
            for way in range(2):
                n = p.steps(j)[way]
                if n:
                    red(j, way, n).wait_recv()
                    ends.append(red_recv.at[way, n - 1, :, spans[j]])

        def layer_rows(core):
            base = pl.ds(pl.multiple_of(p.z * chip_rows + core * my_rows, my_rows), my_rows)
            value = part[base, spans[j]]
            for end in ends:
                value = value + end[part_of(core)].astype(f32)
            moe = value.astype(bf).astype(f32)
            return (after[part_of(core), spans[j]].astype(f32) + moe).astype(bf)

        row_send[:, spans[j]] = layer_rows(1 - c)
        give_rows(j).start()
        out[:, span_of(c, j)] = layer_rows(c)

    def take_rows(j):
        give_rows(j).wait_recv()
        out[:, span_of(1 - c, j)] = row_recv[:, spans[j]]

    down(0)
    for j in range(1, count):
        down(j)
        add_halves(j - 1)
    add_halves(count - 1)
    at = {}

    def advance():
        for j in sorted(at):
            if j == count - 1:
                if at[j] == 1:
                    send_far(j)
                elif at[j] == last:
                    finish(j)
            elif at[j] <= last:
                step(j, at[j])
            elif at[j] == last + 1:
                finish(j)
            at[j] += 1

    for j in range(count):
        blend_rows(j)
        at[j] = 1
        advance()
    while min(at[count - 1] + 1, at[count - 2]) <= last + 1:
        advance()
    for j in range(count):
        take_rows(j)

    @pl.when(sends_rim)
    def _():
        for copy in halo:
            copy.wait_send()

    for j in everything:
        swap(j, c).wait_send()
        ring.drain(j)
        gather.drain(j)
        spread.drain(j)
        forward(j).wait_send()
    swap_res(c).wait_send()
    head_total.wait_send()
    swap_square.wait_send()
    for copy in shared_swaps:
        copy.wait_send()
    swap_pre.wait_send()
    for j in range(count):
        give(j).wait_send()
        back.drain(j)
        give_rows(j).wait_send()
        for way in range(2):
            for m in range(1, p.steps(j)[way] + 1 if j < count - 1 else 1):
                red(j, way, m).wait_send()
    scale_total.wait_send()
    for o in range(1, p.nz):
        far(o).wait_send()


def vmem():
    return pl.BlockSpec(memory_space=pltpu.VMEM)


def layer(queries, keys, values, sink, w_out, residual, gain, ids, weights, wg, wu, wd, sg, su, sd):
    nc, cuts = CHUNKS, len(CUTS)
    rows = queries.shape[1]
    my_rows, width = residual.shape
    half, chip_rows = width // 2, 2 * my_rows
    fc = half // nc
    tp_count, sp_count = lax.axis_size("tp"), lax.axis_size("sp")
    experts = sp_count * tp_count // 2
    slots = sp_count * CAP
    hops = tp_count // 4
    hidden_units, units = wg.shape[0], sg.shape[0]
    bf, f32 = jnp.bfloat16, jnp.float32

    def buf(*shape, dtype=bf):
        return pltpu.VMEM(shape, dtype)

    def sems(*shape):
        return [pltpu.SemaphoreType.DMA(shape)] * 2

    anywhere = pl.BlockSpec(memory_space=pl.ANY)
    return pl.pallas_call(
        layer_kernel,
        name="layer",
        out_shape=jax.ShapeDtypeStruct((my_rows, width), bf),
        in_specs=[vmem()] * 9 + [anywhere] * 3 + [vmem()] * 3,
        out_specs=vmem(),
        scratch_shapes=[
            buf(rows + WINDOW, 128),
            buf(rows + WINDOW, 128),
            buf(rows // WINDOW, HD, WINDOW),
            buf(tp_count * HD, chip_rows),
            buf(chip_rows, tp_count * HD),
            buf(nc, tp_count * HD, fc),
            buf(chip_rows, half),
            buf(chip_rows, half),
            buf(chip_rows, 128, dtype=f32),
            buf(chip_rows, 128, dtype=f32),
            buf(rows, experts),
            buf(experts, rows),
            buf(rows, experts),
            buf(slots, rows),
            buf(rows, slots),
            buf(tp_count // 2, 8, chip_rows, dtype=f32),
            buf(rows, 128, dtype=f32),
            buf(slots, 128, dtype=f32),
            buf(nc, rows, fc),
            buf(slots, half),
            buf(slots, half),
            buf(slots, half),
            buf(hidden_units, width),
            buf(hidden_units, width),
            buf(slots, hidden_units, dtype=f32),
            buf(slots, hidden_units, dtype=f32),
            buf(4 * units, half),
            buf(rows, 4 * units, dtype=f32),
            buf(rows, 4 * units, dtype=f32),
            buf(slots, hidden_units),
            buf(rows, 2 * units),
            buf(hidden_units, width),
            buf(slots, half),
            buf(slots, half),
            buf(slots, half),
            buf(slots, half),
            buf(2 * units, half),
            buf(rows, half, dtype=f32),
            buf(2, hops, chip_rows, half),
            buf(2, hops, chip_rows, half),
            buf(tp_count // 2 - 1, chip_rows, half // sum(CUTS) * CUTS[-1]),
            buf(tp_count // 2 - 1, chip_rows, half // sum(CUTS) * CUTS[-1]),
            buf(my_rows, half),
            buf(my_rows, half),
            pltpu.SemaphoreType.DMA((3,)),
            *sems(2),
            *sems(1),
            *sems(nc),
            *sems(nc, 2, hops),
            *sems(1),
            *sems(1),
            *sems(nc, 2, hops),
            *sems(nc),
            *sems(nc),
            *sems(3),
            *sems(1),
            *sems(cuts),
            *sems(cuts),
            *sems(cuts, 2, hops),
            *sems(cuts),
            *sems(1),
            *sems(tp_count // 2 - 1),
        ],
        compiler_params=pltpu.CompilerParams(
            collective_id=1, has_side_effects=True, vmem_limit_bytes=66_000_000
        ),
    )(queries, keys, values, sink, w_out, residual, gain, ids, weights, wg, wu, wd, sg, su, sd)


def body(
    queries,
    keys,
    values,
    sink_logits,
    w_out,
    residual,
    norm_gain,
    expert_ids,
    expert_weights,
    w_gate,
    w_up,
    w_down,
    shared_gate,
    shared_up,
    shared_down,
):
    return layer(
        queries.T,
        keys,
        values,
        sink_logits[:, None],
        w_out,
        residual,
        norm_gain[None, :],
        expert_ids.T,
        expert_weights.T,
        w_gate[0],
        w_up[0],
        w_down[0],
        shared_gate,
        shared_up,
        shared_down,
    )


def solution(mesh):
    return jax.shard_map(
        body,
        mesh=mesh,
        in_specs=(
            P("sp", "tp"),
            P("sp", None),
            P("sp", None),
            P("tp"),
            P("tp", None),
            P(("sp", "tp"), None),
            P(),
            P("sp", None),
            P("sp", None),
            P(("sp", "tp"), None, None),
            P(("sp", "tp"), None, None),
            P(("sp", "tp"), None, None),
            P("tp", None),
            P("tp", None),
            P("tp", None),
        ),
        out_specs=P(("sp", "tp"), None),
        check_vma=False,
    )
```

time: 362 us -> 155 us (0.43)
  waiting for transfers between devices: 173 us -> 0 us
  Pallas kernels: 0 us -> 153 us
  local copies, waits for them, and re-layouts: 73.6 us -> 1.67 us
  matrix products: 38.2 us -> 0 us
  starting transfers between devices: 20.2 us -> 0 us
  other arithmetic: 20 us -> 0 us
  blocking collectives: 19.9 us -> 0 us
  between operations: 14.2 us -> 0.66 us
    pallas_call x0 -> x1, Pallas kernels: none -> 153 us  [layer(): pl.pallas_call(layer_kernel, name='layer', out_shape=jax.ShapeDtypeStruct...]
    all_to_all x2 -> x0, waiting for transfers between devices: 85 us -> none  [the longest x1 62.8 us: body(): lax.all_to_all(outgoing.reshape(sp_count, capacity, -1), 'sp', split_axis...]
    reduce_scatter x1 -> x0, waiting for transfers between devices: 56.6 us -> none  [body(): lax.psum_scatter(partial_sum.astype(jnp.bfloat16), 'tp', scatter_dimensio...]
    dot_general x7 -> x0, matrix products: 38.2 us -> none  [the longest x1 12.4 us: body(): jnp.dot(hidden, w_down[0], preferred_element_type=jnp.float32)]
    gather x5 -> x0, local copies, waits for them, and re-layouts: 35.7 us -> none  [the longest x4 24.1 us: body(): held[position[:, route_slot]].astype(jnp.float32)]
    all_gather x2 -> x0, waiting for transfers between devices: 26.6 us -> none  [the longest x1 14.4 us: body(): lax.all_gather(w_out, 'tp', axis=0, tiled=True)]
    all_to_all x1 -> x0, blocking collectives: 19.9 us -> none  [body(): lax.all_to_all(attended, 'tp', split_axis=0, concat_axis=1, tiled=True)]
    scatter x1 -> x0, local copies, waits for them, and re-layouts: 15.5 us -> none  [slot_layout(): jnp.full((expert_count * capacity,), -1, jnp.int32).at[slot_index]]
  transfers between devices with their start and end apart: 8 -> 0, of which waited for: 6 -> 0; matrix products, arithmetic and copies ran while one was open for 12% -> 0% of each run, Pallas kernels for 0% -> 0%
where the time goes in v3:
time: 155 us
  Pallas kernels  153 us (99%)
  local copies, waits for them, and re-layouts  1.67 us (1%)
    pallas_call x1, Pallas kernels, layer(): pl.pallas_call(layer_kernel, name='layer', out_shape=jax.ShapeDtypeStruct...  153 us

profile of v3, /device:TPU:1, one launch (start us, length us, event | category | flops | bytes accessed | tf_op | source)
XLA Modules:
  0.0 155.3 jit_solution(12560392918338944202)
XLA Ops:
  0.7 153.0 %layer.1 = bf16[64,2048]{1,0:T(8,128)(2,1)} custom-call(bf16[64,1024]{1,0:T(8,128)(2,1)} %bitcast.12, bf16[1024,256]{1,0:T(8,128)(2,1)} %keys.1, bf16[1024,256]{1,0:T(8,128)(2,1)} %values.1, f32[1,1]{1,0:T(1,128)} %bitcast.8.sink, bf16[64,2048]{1,0:T(8,128)(2,1)} %w_out.1, bf16[64,2048]{1,0:T(8,128)(2,1)} %residual.1, f32[1,2048]{1,0:T(1,128)} %bitcast.15, ...), custom_call_target="tpu_custom_call" | custom-call | tf_op jit(solution)/shard_map/layer/pallas_call | solution.py:693
  153.7 1.7 %copy.18 = bf16[64,2048]{1,0:T(8,128)(2,1)} copy(bf16[64,2048]{1,0:T(8,128)(2,1)} %layer.1) | data formatting | bytes 524288

commit v4 on v3

--- a/solution.py
+++ b/solution.py
@@ -13,6 +13,8 @@
 
 MESH = pl.DeviceIdType.MESH
 CHUNKS = 4
+TALL = 512
+FAR = True
 CUTS = (2, 2, 2, 1, 1)
 CAP = 64
 
@@ -170,6 +172,7 @@
     capacity = slots // p.sp_count
     units = sg.shape[0]
     tile = min(256, rows, slots)
+    tall = min(TALL, rows, slots)
     last = p.nz // 2
     everything = tuple(range(nc))
     kv = p.t // GROUP
@@ -231,18 +234,20 @@
     for j in everything:
         wide[j, shard(c)] = w_out[:, cols(c, j)]
     ring = RingGather(p, wide, 2 * head_rows, o_send, o_recv)
-    for j in everything:
-        swap(j, 1 - c).wait_recv()
-        ring.send(j, 1)
-    hops = iter([(j, k) for k in range(1, last) for j in everything])
+    first, second = (0, 1), (2, 3)
+    turns = sorted([(2 * k, first, k) for k in range(last)] + [(2 * k + 3, second, k) for k in range(last)])
+    hops = [(j, k) for _, pair, k in turns for j in pair]
 
     def hop(count=1):
-        for _ in range(count):
-            event = next(hops, None)
-            if event is not None:
-                ring.wait(*event)
-                ring.send(event[0], event[1] + 1)
-
+        for _ in range(min(count, len(hops))):
+            j, k = hops.pop(0)
+            if k:
+                ring.wait(j, k)
+            else:
+                swap(j, 1 - c).wait_recv()
+            ring.send(j, k + 1)
+
+    hop(2)
     key_ext[pl.ds(WINDOW, rows)] = keys[:, kv_cols]
     value_ext[pl.ds(WINDOW, rows)] = values[:, kv_cols]
     res[part_of(c)] = residual[:, half_of(c)]
@@ -313,7 +318,7 @@
     quarter = max(1, blocks // 4)
     for i in range(0, blocks, quarter):
         attend_some(i, quarter)
-        hop(1 if i == 0 else 2)
+        hop((1, 3, 2, 2)[i // quarter])
 
     shift = capacity.bit_length() - 1
 
@@ -369,15 +374,15 @@
         for i in range(first, end):
             fill_blend(pl.ds(i * tile, tile))
 
-    hop(nc * last)
+    hop(len(hops) - 2)
 
     head_total.wait_recv()
     heads_t[...] = heads[...].T
     swap_res(1 - c).wait_recv()
     chip_place = pl.ds(pl.multiple_of(p.z * chip_rows, chip_rows), chip_rows)
     gather = RingGather(p, ring_buf, chip_rows, g_send, g_recv)
-    squares = jnp.zeros((chip_rows, 1), f32)
-    for j in everything:
+
+    def project(j):
         ring.wait(j, last)
         piece = pl.ds(j * fc, fc)
         mixed = (res[:, piece].astype(f32) + dot_nn(heads_t[...], wide[j])).astype(bf)
@@ -385,11 +390,21 @@
         ring_buf[j, chip_place] = mixed
         gather.send(j, 1)
         mixed = mixed.astype(f32)
-        squares = squares + jnp.sum(mixed * mixed, axis=1, keepdims=True)
+        return jnp.sum(mixed * mixed, axis=1, keepdims=True)
+
+    def pass_on(pair, k):
+        for j in pair if k < last else ():
+            gather.wait(j, k)
+            gather.send(j, k + 1)
+
+    squares = project(0) + project(1)
+    hop(2)
+    pass_on(first, 1)
+    squares = squares + project(2) + project(3)
     square[...] = jnp.broadcast_to(squares, square.shape)
     swap_square = remote(square, square_other, q_send.at[0], q_recv.at[0], p.partner)
     swap_square.start()
-    fill_blend_tiles(0, 1)
+    pass_on(first, 2)
     swap_square.wait_recv()
     mean = (square[...] + square_other[...]) / width
     scale_rows[p.z] = lax.rsqrt(mean + 1e-06).T[:8]
@@ -422,11 +437,6 @@
     def forward(j):
         return remote(own.at[:, even[j]], other.at[:, even[j]], f_send.at[j], f_recv.at[j], p.partner)
 
-    def pass_on(pair, k):
-        for j in pair:
-            gather.wait(j, k)
-            gather.send(j, k + 1)
-
     def select(j):
         gather.wait(j, last)
 
@@ -434,7 +444,7 @@
             value = dot_nn(pick[r], ring_buf[j]) * scale_slots[r][:, :1] * gain[:, cols(c, j)]
             outgoing[r, even[j]] = value.astype(bf)
 
-        rows_loop(slots, tile, one)
+        rows_loop(slots, tall, one)
         spread.send(j)
 
     def shared_part(j):
@@ -453,24 +463,24 @@
         forward(j).wait_recv()
 
         def one(r):
-            a, b = own[r, even[j]], other[r, even[j]]
+            both = jnp.concatenate([own[r, even[j]], other[r, even[j]]], axis=1)
             for w, acc in ((wg, gate_sum), (wu, up_sum)):
-                value = dot_nt(a, w[:, cols(c, j)]) + dot_nt(b, w[:, cols(1 - c, j)])
+                across = jnp.concatenate([w[:, cols(c, j)], w[:, cols(1 - c, j)]], axis=1)
+                value = dot_nt(both, across)
                 acc[r] = value if j == 0 else acc[r] + value
 
-        rows_loop(slots, tile, one)
-
-    for k in range(1, last):
-        pass_on(everything, k)
-        if k == 1:
-            fill_blend_tiles(1, rows // tile)
-            take_scales()
-    if last == 1:
-        fill_blend_tiles(1, rows // tile)
-        take_scales()
+        rows_loop(slots, tall, one)
+
+    fill_blend_tiles(0, rows // tile)
+    pass_on(second, 1)
+    pass_on(first, 3)
     for copy in shared_swaps:
         copy.wait_recv()
-    for j in everything:
+    pass_on(second, 2)
+    take_scales()
+    select(0)
+    pass_on(second, 3)
+    for j in (1, 2, 3):
         select(j)
     for j in (0, 1):
         shared_part(j)
@@ -507,6 +517,7 @@
     sizes = [cut * unit for cut in CUTS]
     spans = [pl.ds(a, n) for a, n in zip(starts, sizes)]
     count = len(CUTS)
+    direct = count - 1 if FAR else None
     back = Exchange(p, total, held, capacity, spans, b_send, b_recv)
 
     def span_of(h, j):
@@ -522,9 +533,9 @@
         def ours(r):
             total[r, spans[j]] = dot_nn(hidden[r], wd[:, span_of(c, j)]).astype(bf)
 
-        rows_loop(slots, tile, theirs)
+        rows_loop(slots, tall, theirs)
         give(j).start()
-        rows_loop(slots, tile, ours)
+        rows_loop(slots, tall, ours)
 
     def add_halves(j):
         give(j).wait_recv()
@@ -543,7 +554,7 @@
             mixed = dot_nn(blend[r], held[:, spans[j]])
             part[r, spans[j]] = mixed + dot_nn(shared[r], sdh[:, spans[j]])
 
-        rows_loop(rows, tile, one)
+        rows_loop(rows, tall, one)
 
     def chip_block(distance):
         index = (p.z + distance + p.nz) % p.nz
@@ -572,7 +583,7 @@
         return remote(far_send.at[o - 1], far_recv.at[o - 1], z_send.at[o - 1], z_recv.at[o - 1], device)
 
     def send_far(j):
-        for o in (o for o in sorted(range(1, p.nz), key=lambda o: -min(o, p.nz - o))):
+        for o in sorted(range(1, p.nz), key=lambda o: -min(o, p.nz - o)):
             far_send[o - 1] = part[chip_block(o), spans[j]].astype(bf)
             far(o).start()
 
@@ -581,7 +592,7 @@
 
     def finish(j):
         ends = []
-        if j == count - 1:
+        if j == direct:
             for o in range(1, p.nz):
                 far(o).wait_recv()
                 ends.append(far_recv.at[o - 1])
@@ -617,7 +628,7 @@
 
     def advance():
         for j in sorted(at):
-            if j == count - 1:
+            if j == direct:
                 if at[j] == 1:
                     send_far(j)
                 elif at[j] == last:
@@ -632,7 +643,7 @@
         blend_rows(j)
         at[j] = 1
         advance()
-    while min(at[count - 1] + 1, at[count - 2]) <= last + 1:
+    while any(at[j] <= last + (j != direct) for j in at):
         advance()
     for j in range(count):
         take_rows(j)
@@ -659,10 +670,10 @@
         back.drain(j)
         give_rows(j).wait_send()
         for way in range(2):
-            for m in range(1, p.steps(j)[way] + 1 if j < count - 1 else 1):
+            for m in range(1, p.steps(j)[way] + 1 if j != direct else 1):
                 red(j, way, m).wait_send()
     scale_total.wait_send()
-    for o in range(1, p.nz):
+    for o in range(1, p.nz if FAR else 1):
         far(o).wait_send()
 
 

time: 155 us -> 149 us (0.961)
  Pallas kernels: 153 us -> 146 us
    pallas_call x1, Pallas kernels: 153 us -> 146 us  [layer(): pl.pallas_call(layer_kernel, name='layer', out_shape=jax.ShapeDtypeStruct...]
where the time goes in v4:
time: 149 us
  Pallas kernels  146 us (98%)
  local copies, waits for them, and re-layouts  1.67 us (1%)
    pallas_call x1, Pallas kernels, layer(): pl.pallas_call(layer_kernel, name='layer', out_shape=jax.ShapeDtypeStruct...  146 us

profile of v4, /device:TPU:1, one launch (start us, length us, event | category | flops | bytes accessed | tf_op | source)
XLA Modules:
  0.0 148.7 jit_solution(13257938398358064481)
XLA Ops:
  0.7 146.4 %layer.1 = bf16[64,2048]{1,0:T(8,128)(2,1)} custom-call(bf16[64,1024]{1,0:T(8,128)(2,1)} %bitcast.12, bf16[1024,256]{1,0:T(8,128)(2,1)} %keys.1, bf16[1024,256]{1,0:T(8,128)(2,1)} %values.1, f32[1,1]{1,0:T(1,128)} %bitcast.8.sink, bf16[64,2048]{1,0:T(8,128)(2,1)} %w_out.1, bf16[64,2048]{1,0:T(8,128)(2,1)} %residual.1, f32[1,2048]{1,0:T(1,128)} %bitcast.15, ...), custom_call_target="tpu_custom_call" | custom-call | tf_op jit(solution)/shard_map/layer/pallas_call | solution.py:704
  147.1 1.7 %copy.18 = bf16[64,2048]{1,0:T(8,128)(2,1)} copy(bf16[64,2048]{1,0:T(8,128)(2,1)} %layer.1) | data formatting | bytes 524288

commit v5 on v4

--- a/solution.py
+++ b/solution.py
@@ -32,7 +32,7 @@
         fn(pl.ds(pl.multiple_of(i * step, step), step))
         return carry
 
-    lax.fori_loop(0, total // step, one, 0)
+    lax.fori_loop(0, total // step, one, 0, unroll=total == 2 * step)
 
 
 class Place:

time: 149 us -> 151 us (1.013)
  Pallas kernels: 146 us -> 149 us
    pallas_call x1, Pallas kernels: 146 us -> 149 us  [layer(): pl.pallas_call(layer_kernel, name='layer', out_shape=jax.ShapeDtypeStruct...]
where the time goes in v5:
time: 151 us
  Pallas kernels  149 us (99%)
  local copies, waits for them, and re-layouts  1.67 us (1%)
    pallas_call x1, Pallas kernels, layer(): pl.pallas_call(layer_kernel, name='layer', out_shape=jax.ShapeDtypeStruct...  149 us

profile of v5, /device:TPU:1, one launch (start us, length us, event | category | flops | bytes accessed | tf_op | source)
XLA Modules:
  0.0 151.1 jit_solution(7623342258527596994)
XLA Ops:
  0.7 148.8 %layer.1 = bf16[64,2048]{1,0:T(8,128)(2,1)} custom-call(bf16[64,1024]{1,0:T(8,128)(2,1)} %bitcast.12, bf16[1024,256]{1,0:T(8,128)(2,1)} %keys.1, bf16[1024,256]{1,0:T(8,128)(2,1)} %values.1, f32[1,1]{1,0:T(1,128)} %bitcast.8.sink, bf16[64,2048]{1,0:T(8,128)(2,1)} %w_out.1, bf16[64,2048]{1,0:T(8,128)(2,1)} %residual.1, f32[1,2048]{1,0:T(1,128)} %bitcast.15, ...), custom_call_target="tpu_custom_call" | custom-call | tf_op jit(solution)/shard_map/layer/pallas_call | solution.py:704
  149.5 1.7 %copy.18 = bf16[64,2048]{1,0:T(8,128)(2,1)} copy(bf16[64,2048]{1,0:T(8,128)(2,1)} %layer.1) | data formatting | bytes 524288
